TPU v7x, 32 devices: a whole 2x2x4 slice. The times are simulated.
32 devices in a mesh: fs: 16 (over z, y, core), tp: 2 (over x).
Axes of the slice: x: 2, y: 2, z: 4, core: 2. Of those that a mesh axis runs over, the one named last changes fastest.
Arguments:
- tokens: bfloat16 [6144, 2048], P('fs', 'tp'), may hold values from -60 to 60
- gain_mixer: float32 [2048], P('tp'), may hold values from 0.1 to 1.9
- w_in: bfloat16 [2048, 1024], P('fs', 'tp'), may hold values from -0.125 to 0.125
- pool_scale: float32 [1024], P('tp'), may hold values from 0.1 to 1.9
- w_pool_out: bfloat16 [2048, 1024], P('fs', 'tp'), may hold values from -0.25 to 0.25
- gain_mid: float32 [2048], P('tp'), may hold values from 0.1 to 1.9
- w_ff1: bfloat16 [2048, 8192], P('fs', 'tp'), may hold values from -0.125 to 0.125
- w_ff2: bfloat16 [2048, 8192], P('fs', 'tp'), may hold values from -0.09375 to 0.09375
- gain_out: float32 [2048], P('tp'), may hold values from 0.1 to 1.9
Outputs:
- layer_out: bfloat16 [6144, 2048], P('fs', 'tp')
All inputs are finite; a program needn't handle non-finite values.
Results may differ from a plain program's by a relative error of at most 0.017.
Values may be sent and summed in bfloat16 or wider, within the bound.
A program may use at most 128 MiB of HBM per device.

v0:
```python
import functools
import math

import jax
import jax.numpy as jnp
from jax import lax
from jax.experimental import pallas as pl
from jax.experimental.pallas import tpu as pltpu
from jax.sharding import PartitionSpec as P

norm_eps = 1e-05
residual_alpha = 2.0**0.25
f32, bf16 = jnp.float32, jnp.bfloat16
MESH = pl.DeviceIdType.MESH


def nt_dot(left, right):
    return lax.dot_general(left, right, (((1,), (1,)), ((), ())), preferred_element_type=f32)


def kernel(
    n, tps,
    x_ref, gains_ref, scale_ref, gout_ref, win_ref, wpo_ref, wup_ref, wdn_ref, out_ref,
    win, wpo, wup, wdn, xfull, gfull, mixed, mpart, mrecv, middle, hidden, part, precv, work,
    load_sem, is_sem, ir_sem, ds_sem, dr_sem, xs_sem, xr_sem, gs_sem, gr_sem,
    ms_sem, mr_sem, ps_sem, pr_sem,
):
    i, t = lax.axis_index("fs"), lax.axis_index("tp")
    core, chip = lax.rem(i, 2), lax.div(i, 2)
    half = n // 2
    rows, feat = x_ref.shape
    cin = win_ref.shape[1]
    width = feat * tps
    own = win_ref.shape[0]
    rh = own // 2
    rc = own * 2
    ffw = wup_ref.shape[1]
    fh = ffw // 2

    pos = jnp.where(lax.rem(chip, 2) == 0, lax.div(chip, 2), n - 1 - lax.div(chip, 2))

    def chip_at(p):
        q = lax.rem(p + 2 * n, n)
        return jnp.where(q < half, 2 * q, 2 * (n - 1 - q) + 1)

    sib = chip * 2 + (1 - core)
    ring = [chip_at(pos + 1) * 2 + core, chip_at(pos - 1) * 2 + core]
    peers = [lax.rem(t + q, tps) for q in range(1, tps)]

    streams = [(win, 0, cin), (wpo, 0, cin), (wup, 0, fh), (wup, fh, fh), (wdn, 0, fh), (wdn, fh, fh)]

    def block(w, where, c, d):
        ref, c0, cw = streams[w]
        r0 = pl.multiple_of((where * 2 + c) * own + d * rh, rh)
        return ref.at[pl.ds(r0, rh), pl.ds(c0, cw)]

    def source(s, d):
        return chip_at(pos - s) if d == 0 else chip_at(pos + s)

    def hop(w, s, d):
        b = block(w, source(s, d), core, d)
        return pltpu.make_async_remote_copy(
            b, b, is_sem.at[w, s, d], ir_sem.at[w, s, d], device_id=(ring[d], t), device_id_type=MESH)

    def share(w, s, d):
        b = block(w, source(s, d), core, d)
        return pltpu.make_async_remote_copy(
            b, b, ds_sem.at[w, s, d], dr_sem.at[w, s, d], device_id=(sib, t), device_id_type=MESH)

    def begin(w):
        for d in range(2):
            hop(w, 0, d).start()
        for d in range(2):
            share(w, 0, d).start()

    def advance(ws, s, last=False):
        for w in ws:
            for d in range(2):
                hop(w, s, d).wait_recv()
                if not last:
                    hop(w, s + 1, d).start()
                share(w, s + 1, d).start()

    def run(ws, lo, hi):
        def body(s, carry):
            advance(ws, s)
            return carry
        lax.fori_loop(lo, hi, body, 0)

    def shared(w):
        def body(s, carry):
            for d in range(2):
                share(w, s, d).wait_recv()
            return carry
        lax.fori_loop(0, n, body, 0)

    barrier = pltpu.get_barrier_semaphore()
    for f in ring + [sib]:
        pl.semaphore_signal(barrier, inc=1, device_id=(f, t), device_id_type=MESH)
    for p in peers:
        pl.semaphore_signal(barrier, inc=1, device_id=(i, p), device_id_type=MESH)
    loads = []
    mine = pl.ds(pl.multiple_of(i * own, own), own)
    for k, (src, dst) in enumerate(((win_ref, win), (wpo_ref, wpo), (wup_ref, wup), (wdn_ref, wdn))):
        loads.append(pltpu.make_async_copy(src, dst.at[mine], load_sem.at[k]))
        loads[-1].start()
    pl.semaphore_wait(barrier, 3 + len(peers))

    def x_copy(q):
        return pltpu.make_async_remote_copy(
            x_ref, xfull.at[t], xs_sem.at[q], xr_sem.at[q], device_id=(i, peers[q]), device_id_type=MESH)

    def g_copy(q):
        return pltpu.make_async_remote_copy(
            gains_ref, gfull.at[t], gs_sem.at[q], gr_sem.at[q], device_id=(i, peers[q]), device_id_type=MESH)

    for w in range(2):
        loads[w].wait()
        begin(w)
    for q in range(tps - 1):
        x_copy(q).start()
        g_copy(q).start()
    xfull[t] = x_ref[...]
    gfull[t] = gains_ref[...]

    run((0, 1), 0, n - 2)
    loads[2].wait()
    begin(2)
    begin(3)
    advance((0, 1), n - 2, last=True)
    loads[3].wait()

    rb = math.gcd(rows, 32)

    def blocks_of(body):
        def step(r, carry):
            body(pl.ds(pl.multiple_of(r * rb, rb), rb))
            return carry
        lax.fori_loop(0, rows // rb, step, 0)

    def norm(pieces):
        total = sum(jnp.sum(v, axis=1, keepdims=True) for v in pieces)
        mean = total / width
        pieces = [v - mean for v in pieces]
        spread = sum(jnp.sum(v * v, axis=1, keepdims=True) for v in pieces) / width
        inv = lax.rsqrt(spread + norm_eps)
        return [v * inv for v in pieces]

    for q in range(tps - 1):
        x_copy(q).wait_recv()
        g_copy(q).wait_recv()

    def first_norm(rs):
        pieces = norm([xfull[r, rs, :].astype(f32) for r in range(tps)])
        for r in range(tps):
            mixed[rs, r * feat:(r + 1) * feat] = (pieces[r] * gfull[r, 0:1, :]).astype(bf16)

    blocks_of(first_norm)
    shared(0)
    cb = math.gcd(cin, 128)
    gw = cin * tps // 4
    pool = jnp.dot(mixed[...], win[...], preferred_element_type=f32)
    work[:, :cin] = pool.astype(bf16).astype(f32)
    row = lax.broadcasted_iota(jnp.int32, (rows, cb), 0)
    position = (row + 1).astype(f32)
    pooled = []
    for c in range(cin // cb):
        cs = slice(c * cb, (c + 1) * cb)
        u = work[:, cs]

        def shifted(v, steps):
            return jnp.where(row >= steps, pltpu.roll(v, steps, axis=0), 0.0)

        s2 = u + shifted(u, 1)
        s4 = s2 + shifted(s2, 2)
        s8 = s4 + shifted(s4, 4)
        s16 = s8 + shifted(s8, 8)
        channel = t * cin + c * cb + lax.broadcasted_iota(jnp.int32, (rows, cb), 1)

        def pick(a, b, e, g):
            return jnp.where(channel < gw, a, jnp.where(channel < 2 * gw, b, jnp.where(channel < 3 * gw, e, g)))

        count = jnp.minimum(position, pick(2.0, 4.0, 8.0, 16.0))
        mixed[:, cs] = ((pick(s2, s4, s8, s16) / count - u) * scale_ref[0:1, cs]).astype(bf16)

    def m_copy(q):
        return pltpu.make_async_remote_copy(
            mpart, mrecv.at[q], ms_sem.at[q], mr_sem.at[q], device_id=(i, peers[q]), device_id_type=MESH)

    shared(1)
    wb = math.gcd(width, 512)

    def out_proj(k, carry):
        cs = pl.ds(pl.multiple_of(k * wb, wb), wb)
        mpart[:, cs] = nt_dot(mixed[:, :cin], wpo[cs, :]).astype(bf16)
        return carry

    lax.fori_loop(0, width // wb, out_proj, 0)
    for q in range(tps - 1):
        m_copy(q).start()

    run((2, 3), 0, half)
    for q in range(tps - 1):
        m_copy(q).wait_recv()

    def second_norm(rs):
        pieces = []
        for r in range(tps):
            cs = slice(r * feat, (r + 1) * feat)
            mix = mpart[rs, cs].astype(f32)
            for q in range(tps - 1):
                mix = mix + mrecv[q, rs, cs].astype(f32)
            mix = mix.astype(bf16).astype(f32)
            pieces.append(residual_alpha * xfull[r, rs, :].astype(f32) + mix)
        pieces = norm(pieces)
        for r in range(tps):
            middle[rs, r * feat:(r + 1) * feat] = (pieces[r] * gfull[r, 1:2, :]).astype(bf16)

    blocks_of(second_norm)
    run((2, 3), half, n - 2)
    begin(4)
    begin(5)
    advance((2, 3), n - 2, last=True)
    shared(2)
    shared(3)

    hb = math.gcd(ffw, 512)
    chunks = ffw // hb

    def up(k, carry):
        cs = pl.ds(pl.multiple_of(k * hb, hb), hb)
        act = jnp.maximum(jnp.dot(middle[...], wup[:, cs], preferred_element_type=f32), 0.0)
        hidden[:, cs] = (act * act).astype(bf16)
        return carry

    third = -(-chunks // 3)
    lax.fori_loop(0, third, up, 0)
    advance((4,), 0)
    lax.fori_loop(third, min(2 * third, chunks), up, 0)
    advance((5,), 0)
    lax.fori_loop(min(2 * third, chunks), chunks, up, 0)

    def p_copy(q, k):
        return pltpu.make_async_remote_copy(
            part.at[k], precv.at[q, k], ps_sem.at[q, k], pr_sem.at[q, k],
            device_id=(i, peers[q]), device_id_type=MESH)

    def down(distance):
        for w in (4, 5):
            share(w, distance, 0).wait_recv()
            share(w, lax.rem(n - distance, n), 1).wait_recv()
        k = chip_at(pos - distance)
        part[k] = nt_dot(hidden[...], wdn[pl.ds(pl.multiple_of(k * rc, rc), rc), :]).astype(bf16)
        for q in range(tps - 1):
            p_copy(q, k).start()

    advance((4, 5), 1)
    run((4, 5), 2, half - 1)

    def first_two(j, carry):
        down(j * half)
        return carry

    def last_two(s):
        def body(j, carry):
            down(jnp.where(j == 0, s + 1, n - 1 - s))
            return carry
        lax.fori_loop(0, 2, body, 0)

    advance((4, 5), half - 1)
    lax.fori_loop(0, 2, first_two, 0)

    def tail(s, carry):
        advance((4, 5), s)
        last_two(s)
        return carry

    lax.fori_loop(half, n - 2, tail, 0)
    advance((4, 5), n - 2, last=True)
    last_two(n - 2)

    for q in range(tps - 1):
        def arrived(k, carry):
            p_copy(q, k).wait_recv()
            return carry
        lax.fori_loop(0, n, arrived, 0)

    per = n // tps

    def last_norm(rs):
        total = jnp.zeros((rb, 1), f32)
        values = []
        for k in range(n):
            ff = part[k, rs, :].astype(f32)
            for q in range(tps - 1):
                ff = ff + precv[q, k, rs, :].astype(f32)
            v = residual_alpha * middle[rs, k * rc:(k + 1) * rc].astype(f32) + ff.astype(bf16).astype(f32)
            values.append(v)
            total = total + jnp.sum(v, axis=1, keepdims=True)
        mean = total / width
        square = jnp.zeros((rb, 1), f32)
        for v in values:
            square = square + jnp.sum((v - mean) * (v - mean), axis=1, keepdims=True)
        inv = lax.rsqrt(square / width + norm_eps)
        for j in range(per):
            v = values[j]
            for r in range(1, tps):
                v = jnp.where(t == r, values[r * per + j], v)
            cs = slice(j * rc, (j + 1) * rc)
            out_ref[rs, cs] = ((v - mean) * inv * gout_ref[0:1, cs]).astype(bf16)

    blocks_of(last_norm)

    for q in range(tps - 1):
        x_copy(q).wait_send()
        g_copy(q).wait_send()
        m_copy(q).wait_send()

        def sent(k, carry):
            p_copy(q, k).wait_send()
            return carry
        lax.fori_loop(0, n, sent, 0)

    def drained(s, carry):
        for w in range(len(streams)):
            for d in range(2):
                hop(w, s, d).wait_send()
                share(w, s, d).wait_send()
        return carry

    lax.fori_loop(0, n - 1, drained, 0)
    for w in range(len(streams)):
        for d in range(2):
            share(w, n - 1, d).wait_send()


def local(n, tps, tokens, gain_mixer, w_in, pool_scale, w_pool_out, gain_mid, w_ff1, w_ff2, gain_out):
    rows, feat = tokens.shape
    own, cin = w_in.shape
    ffw = w_ff1.shape[1]
    width = feat * tps
    rc = own * 2
    gains = jnp.stack([gain_mixer, gain_mid])
    vmem, hbm = pl.BlockSpec(memory_space=pltpu.VMEM), pl.BlockSpec(memory_space=pl.ANY)
    dma = pltpu.SemaphoreType.DMA
    lanes = tps - 1
    return pl.pallas_call(
        functools.partial(kernel, n, tps),
        out_shape=jax.ShapeDtypeStruct((rows, feat), bf16),
        in_specs=[vmem] * 4 + [hbm] * 4,
        out_specs=vmem,
        scratch_shapes=[
            pltpu.VMEM((width, cin), bf16),
            pltpu.VMEM((width, cin), bf16),
            pltpu.VMEM((width, ffw), bf16),
            pltpu.VMEM((width, ffw), bf16),
            pltpu.VMEM((tps, rows, feat), bf16),
            pltpu.VMEM((tps, 2, feat), f32),
            pltpu.VMEM((rows, width), bf16),
            pltpu.VMEM((rows, width), bf16),
            pltpu.VMEM((lanes, rows, width), bf16),
            pltpu.VMEM((rows, width), bf16),
            pltpu.VMEM((rows, ffw), bf16),
            pltpu.VMEM((n, rows, rc), bf16),
            pltpu.VMEM((lanes, n, rows, rc), bf16),
            pltpu.VMEM((rows, cin), f32),
            dma((4,)),
            dma((6, n, 2)), dma((6, n, 2)), dma((6, n, 2)), dma((6, n, 2)),
            dma((lanes,)), dma((lanes,)), dma((lanes,)), dma((lanes,)),
            dma((lanes,)), dma((lanes,)), dma((lanes, n)), dma((lanes, n)),
        ],
        compiler_params=pltpu.CompilerParams(
            collective_id=0, has_side_effects=True, vmem_limit_bytes=67043328
        ),
    )(tokens, gains, pool_scale[None], gain_out[None], w_in, w_pool_out, w_ff1, w_ff2)


def solution(mesh):
    n, tps = mesh.shape["fs"] // 2, mesh.shape["tp"]
    return jax.shard_map(
        functools.partial(local, n, tps),
        mesh=mesh,
        in_specs=(
            P("fs", "tp"),
            P("tp"),
            P("fs", "tp"),
            P("tp"),
            P("fs", "tp"),
            P("tp"),
            P("fs", "tp"),
            P("fs", "tp"),
            P("tp"),
        ),
        out_specs=P("fs", "tp"),
        check_vma=False,
    )
```

profile of v0, /device:TPU:0, one launch (start us, length us, event | category | flops | bytes accessed | tf_op | source)
XLA Modules:
  0.0 211.5 jit_solution(17277805409856340715)
XLA Ops:
  0.0 0.0 copy-start
  0.0 0.7 copy-done
  0.7 1.3 pad_maximum_fusion.gains_ref
  2.0 207.5 %shard_map.91 = bf16[384,1024]{1,0:T(8,128)(2,1)} custom-call(bf16[384,1024]{1,0:T(8,128)(2,1)} %x_ref.1, f32[2,1024]{1,0:T(2,128)} %pad_maximum_fusion.gains_ref, f32[1,512]{1,0:T(1,128)} %bitcast.7, f32[1,1024]{1,0:T(1,128)} %bitcast.6, bf16[128,512]{1,0:T(8,128)(2,1)} %win_ref.1, bf16[128,512]{1,0:T(8,128)(2,1)} %wpo_ref.1, bf16[128,4096]{1,0:T(8,128)(2,1)} %wup_ref.1, ...), custom_call_target="tpu_custom_call" | custom-call | tf_op jit(solution)/shard_map/pallas_call | solution.py:347
  209.5 2.1 copy.11
Async XLA Ops:
  0.0 0.7 copy-start
where the time goes:
time: 212 us
  Pallas kernels  207 us (98%)
  local copies, waits for them, and re-layouts  2.75 us (1%)
    pallas_call x1, Pallas kernels, local(): pl.pallas_call(functools.partial(kernel, n, tps), out_shape=jax.ShapeDtyp...  207 us

commit v1 on v0

v1 whole, which is shorter than its diff:
```python
import functools
import math

import jax
import jax.numpy as jnp
from jax import lax
from jax.experimental import pallas as pl
from jax.experimental.pallas import tpu as pltpu
from jax.sharding import PartitionSpec as P

norm_eps = 1e-05
residual_alpha = 2.0**0.25
f32, bf16 = jnp.float32, jnp.bfloat16
MESH = pl.DeviceIdType.MESH


def nt_dot(left, right):
    return lax.dot_general(left, right, (((1,), (1,)), ((), ())), preferred_element_type=f32)


def kernel(
    zn, tps,
    x_ref, gains_ref, scale_ref, gout_ref, win_ref, wpo_ref, wup_ref, wdn_ref, out_ref,
    win, wpo, wup, wdn, sup, sdn, xfull, gfull, mixed, mpart, mrecv, middle, hidden,
    part, precv, zpart, zrecv, total, moments, spread, stat, srecv, work,
    load_sem, zs_sem, zr_sem, ys_sem, yr_sem, ss_sem, sr_sem, xs_sem, xr_sem, gs_sem, gr_sem,
    ms_sem, mr_sem, as_sem, ar_sem, fs_sem, fr_sem, rs_sem, rr_sem, ps_sem, pr_sem, ts_sem, tr_sem,
):
    i, t = lax.axis_index("fs"), lax.axis_index("tp")
    c = lax.rem(i, 2)
    y = lax.rem(lax.div(i, 2), 2)
    z = lax.div(i, 4)
    role = lax.rem(z, 2)
    rows, feat = x_ref.shape
    cin = win_ref.shape[1]
    width = feat * tps
    own = win_ref.shape[0]
    ffw = wup_ref.shape[1]
    fh = ffw // 2
    fq = fh // 2
    n = zn * 2
    per = n // tps
    rc = own * 2
    hr = rows // 2
    lanes = tps - 1

    def across(j):
        other, bit = z, 1
        while bit < zn:
            if j & bit:
                other = other + bit * (1 - 2 * lax.rem(lax.div(z, bit), 2))
            bit *= 2
        return other

    order = [0]
    for j in range(1, zn // 2 + 1):
        for v in (zn // 2 + j - 1, j):
            if v not in order:
                order.append(v)
    far = order[1:]

    def dev(zz, yy, cc):
        return (zz * 2 + yy) * 2 + cc

    sib = dev(z, y, 1 - c)
    opp = dev(z, 1 - y, c)
    mate = dev(across(1), y, c)
    peers = [lax.rem(t + q, tps) for q in range(1, tps)]
    mine = pl.ds(pl.multiple_of(i * own, own), own)

    WIN, WPO, UP0, UP1, DN = range(5)
    streams = [(win, 0, cin), (wpo, 0, cin), (wup, 0, fq), (wup, fq, fq), (wdn, 0, fh)]

    def block(w, zz, yy, cc):
        ref, c0, cw = streams[w]
        r0 = pl.multiple_of(dev(zz, yy, cc) * own, own)
        return ref.at[pl.ds(r0, own), pl.ds(c0, cw)]

    def remote(src, dst, send, recv, to, tt):
        return pltpu.make_async_remote_copy(
            src, dst, send, recv, device_id=(to, tt), device_id_type=MESH)

    def zsend(w, j):
        zd = across(j)
        ref, c0, cw = streams[w]
        b = block(w, z, y, c)
        if w in (WIN, WPO):
            src = b
        else:
            stage = sdn if w == DN else sup
            src = stage.at[:, pl.ds(pl.multiple_of(lax.rem(zd, 2) * fh + c0, 128), cw)]
        return remote(src, b, zs_sem.at[w, j], zr_sem.at[w, j], dev(zd, y, c), t)

    def yfwd(w, j):
        b = block(w, across(j), y, c)
        return remote(b, b, ys_sem.at[w, j], yr_sem.at[w, j], opp, t)

    def share(w, j, s):
        b = block(w, across(j), y if s == 0 else 1 - y, c)
        return remote(b, b, ss_sem.at[w, j, s], sr_sem.at[w, j, s], sib, t)

    def zsends(w, js):
        for j in js:
            zsend(w, j).start()

    def own_start(w):
        yfwd(w, 0).start()
        share(w, 0, 0).start()

    def z_in(w, j):
        zsend(w, j).wait_recv()
        yfwd(w, j).start()
        share(w, j, 0).start()

    def y_in(w, j):
        yfwd(w, j).wait_recv()
        share(w, j, 1).start()

    def s_in(w):
        for j in order:
            for s in range(2):
                share(w, j, s).wait_recv()

    def x_copy(q):
        return remote(x_ref, xfull.at[t], xs_sem.at[q], xr_sem.at[q], i, peers[q])

    def g_copy(q):
        return remote(gains_ref, gfull.at[t], gs_sem.at[q], gr_sem.at[q], i, peers[q])

    def half(h):
        return pl.ds(h * hr, hr)

    def m_copy(q, h):
        return remote(mpart.at[half(h)], mrecv.at[q, half(h)], ms_sem.at[q, h], mr_sem.at[q, h], i, peers[q])

    slab = pl.ds(pl.multiple_of(t * feat, feat), feat)

    def a_copy(h):
        b = middle.at[role, half(h), slab]
        return remote(b, b, as_sem.at[h], ar_sem.at[h], mate, t)

    def f_copy(q, h):
        b = middle.at[1 - role, half(h), slab]
        return remote(b, b, fs_sem.at[q, h], fr_sem.at[q, h], i, peers[q])

    def slot(s):
        return pl.ds(pl.multiple_of(s * rows, rows), rows)

    def r_copy(g, s):
        holder, gl = lax.div(g, per), lax.rem(g, per)
        q = lax.rem(t - holder - 1 + 2 * tps, tps)
        which = (1 - role) if s == 0 else role
        return remote(
            part.at[g, slot(which)], precv.at[q, gl, slot(which)],
            rs_sem.at[g, s], rr_sem.at[q, gl, s], i, holder)

    def r_wait(q, gl, s):
        which = (1 - role) if s == 0 else role
        b = precv.at[q, gl, slot(which)]
        remote(b, b, rs_sem.at[0, s], rr_sem.at[q, gl, s], i, peers[0]).wait_recv()

    def p_copy(gl):
        return remote(zpart.at[gl], zrecv.at[gl], ps_sem.at[gl], pr_sem.at[gl], mate, t)

    def t_copy(q):
        return remote(stat, srecv.at[q], ts_sem.at[q], tr_sem.at[q], i, peers[q])

    barrier = pltpu.get_barrier_semaphore()
    for f in [dev(across(j), y, c) for j in far] + [opp, sib]:
        pl.semaphore_signal(barrier, inc=1, device_id=(f, t), device_id_type=MESH)
    for p in peers:
        pl.semaphore_signal(barrier, inc=1, device_id=(i, p), device_id_type=MESH)
    part_cols = pl.ds(pl.multiple_of(role * fh, 128), fh)
    loads = [
        pltpu.make_async_copy(win_ref, win.at[mine], load_sem.at[0]),
        pltpu.make_async_copy(wpo_ref, wpo.at[mine], load_sem.at[1]),
        pltpu.make_async_copy(wup_ref, sup, load_sem.at[2]),
        pltpu.make_async_copy(wup_ref.at[:, part_cols], wup.at[mine], load_sem.at[3]),
        pltpu.make_async_copy(wdn_ref, sdn, load_sem.at[4]),
        pltpu.make_async_copy(wdn_ref.at[:, part_cols], wdn.at[mine], load_sem.at[5]),
    ]
    for copy in loads:
        copy.start()
    pl.semaphore_wait(barrier, len(far) + 2 + len(peers))

    for q in range(lanes):
        x_copy(q).start()
        g_copy(q).start()
    loads[0].wait()
    own_start(WIN)
    zsends(WIN, far)
    loads[1].wait()
    own_start(WPO)
    zsends(WPO, far)
    loads[2].wait()
    loads[3].wait()
    zsends(UP0, far)
    xfull[t] = x_ref[...]
    gfull[t] = gains_ref[...]
    loads[4].wait()
    loads[5].wait()

    rb = math.gcd(hr, 32)

    def blocks_of(body, lo=0, hi=rows):
        def step(r, carry):
            body(pl.ds(pl.multiple_of(lo + r * rb, rb), rb))
            return carry
        lax.fori_loop(0, (hi - lo) // rb, step, 0)

    def norm(pieces):
        mean = sum(jnp.sum(v, axis=1, keepdims=True) for v in pieces) / width
        pieces = [v - mean for v in pieces]
        var = sum(jnp.sum(v * v, axis=1, keepdims=True) for v in pieces) / width
        inv = lax.rsqrt(var + norm_eps)
        return [v * inv for v in pieces]

    def first_norm(rs):
        pieces = norm([xfull[r, rs, :].astype(f32) for r in range(tps)])
        for r in range(tps):
            mixed[rs, r * feat:(r + 1) * feat] = (pieces[r] * gfull[r, 0:1, :]).astype(bf16)

    zev = [(WIN, j) for j in far] + [(WPO, j) for j in far]
    yev = [(WIN, 0), (WPO, 0)] + zev
    for k, ev in enumerate(zev):
        z_in(*ev)
        if k >= 1:
            y_in(*yev[k - 1])
        if k == len(far):
            for q in range(lanes):
                x_copy(q).wait_recv()
                g_copy(q).wait_recv()
            blocks_of(first_norm)
    own_start(UP0)
    own_start(UP1)
    zsends(UP1, far)
    rest = yev[len(zev) - 1:]
    for ev in rest:
        if ev[0] == WIN:
            y_in(*ev)
    rest = [ev for ev in rest if ev[0] == WPO]
    s_in(WIN)

    cb = math.gcd(cin, 128)
    gw = cin * tps // 4
    pool = jnp.dot(mixed[...], win[...], preferred_element_type=f32)
    work[:, :cin] = pool.astype(bf16).astype(f32)
    for ev in rest:
        y_in(*ev)
    row = lax.broadcasted_iota(jnp.int32, (rows, cb), 0)
    position = (row + 1).astype(f32)
    for k in range(cin // cb):
        cs = slice(k * cb, (k + 1) * cb)
        u = work[:, cs]

        def shifted(v, steps):
            return jnp.where(row >= steps, pltpu.roll(v, steps, axis=0), 0.0)

        s2 = u + shifted(u, 1)
        s4 = s2 + shifted(s2, 2)
        s8 = s4 + shifted(s4, 4)
        s16 = s8 + shifted(s8, 8)
        channel = t * cin + k * cb + lax.broadcasted_iota(jnp.int32, (rows, cb), 1)

        def pick(a, b, e, g):
            return jnp.where(channel < gw, a, jnp.where(channel < 2 * gw, b, jnp.where(channel < 3 * gw, e, g)))

        count = jnp.minimum(position, pick(2.0, 4.0, 8.0, 16.0))
        mixed[:, cs] = ((pick(s2, s4, s8, s16) / count - u) * scale_ref[0:1, cs]).astype(bf16)

    s_in(WPO)
    wb = math.gcd(width, 512)
    for h in range(2):
        def out_proj(k, carry):
            cs = pl.ds(pl.multiple_of(k * wb, wb), wb)
            mpart[half(h), cs] = nt_dot(mixed[half(h), :cin], wpo[cs, :]).astype(bf16)
            return carry

        lax.fori_loop(0, width // wb, out_proj, 0)
        for q in range(lanes):
            m_copy(q, h).start()

    def second_norm(rs):
        pieces = []
        for r in range(tps):
            cs = slice(r * feat, (r + 1) * feat)
            mix = mpart[rs, cs].astype(f32)
            for q in range(lanes):
                mix = mix + mrecv[q, rs, cs].astype(f32)
            mix = mix.astype(bf16).astype(f32)
            pieces.append(residual_alpha * xfull[r, rs, :].astype(f32) + mix)
        pieces = norm(pieces)
        for r in range(tps):
            middle[role, rs, r * feat:(r + 1) * feat] = (pieces[r] * gfull[r, 1:2, :]).astype(bf16)

    def settle(h):
        for q in range(lanes):
            m_copy(q, h).wait_recv()
        blocks_of(second_norm, h * hr, (h + 1) * hr)
        a_copy(h).start()

    zev = [(UP0, j) for j in far] + [(UP1, j) for j in far]
    yev = [(UP0, 0), (UP1, 0)] + zev
    for k, ev in enumerate(zev):
        z_in(*ev)
        y_in(*yev[k])
        if k == len(far):
            settle(0)
        if k == len(far) + 1:
            own_start(DN)
            zsends(DN, far[:1])
    settle(1)
    zsends(DN, far[1:])
    for ev in yev[len(zev):]:
        y_in(*ev)

    hb = math.gcd(fq, 512)

    def ff1(s, lo, hi):
        def up(k, carry):
            cs = pl.ds(pl.multiple_of(lo + k * hb, hb), hb)
            act = jnp.maximum(jnp.dot(middle[s], wup[:, cs], preferred_element_type=f32), 0.0)
            hidden[slot(s), cs] = (act * act).astype(bf16)
            return carry
        lax.fori_loop(0, (hi - lo) // hb, up, 0)

    def pass_on(h):
        a_back = middle.at[1 - role, half(h), slab]
        remote(a_back, a_back, as_sem.at[h], ar_sem.at[h], mate, t).wait_recv()
        for q in range(lanes):
            f_copy(q, h).start()

    s_in(UP0)
    ff1(role, 0, fq)
    pass_on(0)
    z_in(DN, far[0])
    s_in(UP1)
    ff1(role, fq, fh)
    pass_on(1)
    y_in(DN, 0)
    for h in range(2):
        for q in range(lanes):
            f_copy(q, h).wait_recv()
    ff1(1 - role, 0, fh)

    def down(j, s):
        g = across(j) * 2 + (y if s == 0 else 1 - y)
        share(DN, j, s).wait_recv()
        part[g] = nt_dot(hidden[...], wdn[pl.ds(pl.multiple_of(g * rc, rc), rc), :]).astype(bf16)

        @pl.when(lax.div(g, per) != t)
        def _():
            r_copy(g, 0).start()
            r_copy(g, 1).start()

    def fold(j, s):
        g = across(j) * 2 + (y if s == 0 else 1 - y)
        gl = lax.rem(g, per)

        @pl.when(lax.div(g, per) == t)
        def _():
            for q in range(lanes):
                r_wait(q, gl, 0)
            v = part[g, slot(1 - role), :].astype(f32)
            for q in range(lanes):
                v = v + precv[q, gl, slot(1 - role), :].astype(f32)
            zpart[gl] = v.astype(bf16)
            p_copy(gl).start()

    for k, j in enumerate(order):
        if k + 2 < zn:
            z_in(DN, order[k + 2])
        down(j, 0)
        if k + 1 < zn:
            y_in(DN, order[k + 1])
        down(j, 1)
        if k:
            for s in range(2):
                fold(order[k - 1], s)
    for s in range(2):
        fold(order[-1], s)

    for gl in range(per):
        for q in range(lanes):
            r_wait(q, gl, 1)
        p_copy(gl).wait_recv()

    lane = lax.broadcasted_iota(jnp.int32, (rb, 128), 1)

    def gather_up(rs):
        own_rows = pl.ds(pl.multiple_of(role * rows + rs.start, rb), rb)
        base = middle[role, rs, slab]
        values = []
        mean = jnp.zeros((rb, 1), f32)
        for gl in range(per):
            ff = part[t * per + gl, own_rows, :].astype(f32)
            for q in range(lanes):
                ff = ff + precv[q, gl, own_rows, :].astype(f32)
            ff = (ff + zrecv[gl, rs, :].astype(f32)).astype(bf16).astype(f32)
            v = residual_alpha * base[:, gl * rc:(gl + 1) * rc].astype(f32) + ff
            total[rs, gl * rc:(gl + 1) * rc] = v
            values.append(v)
            mean = mean + jnp.sum(v, axis=1, keepdims=True)
        mean = mean / feat
        square = jnp.zeros((rb, 1), f32)
        for v in values:
            square = square + jnp.sum((v - mean) * (v - mean), axis=1, keepdims=True)
        moments[0, rs, :] = jnp.where(lane == 0, mean, jnp.where(lane == 1, square, 0.0))

    blocks_of(gather_up)
    stat[...] = jnp.transpose(moments[0])[0:8, :]
    for q in range(lanes):
        t_copy(q).start()
    spread[...] = jnp.zeros_like(spread)
    for q in range(lanes):
        t_copy(q).wait_recv()
        spread[0:8, :] = srecv[q]
        moments[q + 1] = jnp.transpose(spread[...])

    def last_norm(rs):
        means = [moments[q, rs, 0:1] for q in range(tps)]
        mean = sum(means) / tps
        square = sum(moments[q, rs, 1:2] for q in range(tps))
        for m in means:
            square = square + feat * (m - mean) * (m - mean)
        inv = lax.rsqrt(square / width + norm_eps)
        out_ref[rs, :] = ((total[rs, :] - mean) * inv * gout_ref[0:1, :]).astype(bf16)

    blocks_of(last_norm)

    for q in range(lanes):
        x_copy(q).wait_send()
        g_copy(q).wait_send()
        t_copy(q).wait_send()
        for h in range(2):
            m_copy(q, h).wait_send()
            f_copy(q, h).wait_send()
    for h in range(2):
        a_copy(h).wait_send()

    def sent(g, carry):
        @pl.when(lax.div(g, per) != t)
        def _():
            r_copy(g, 0).wait_send()
            r_copy(g, 1).wait_send()
        return carry

    lax.fori_loop(0, n, sent, 0)

    def folded(gl, carry):
        p_copy(gl).wait_send()
        return carry

    lax.fori_loop(0, per, folded, 0)
    for w in range(len(streams)):
        for j in order:
            if j:
                zsend(w, j).wait_send()
            yfwd(w, j).wait_send()
            share(w, j, 0).wait_send()
            share(w, j, 1).wait_send()


def local(zn, tps, tokens, gain_mixer, w_in, pool_scale, w_pool_out, gain_mid, w_ff1, w_ff2, gain_out):
    rows, feat = tokens.shape
    own, cin = w_in.shape
    ffw = w_ff1.shape[1]
    fh = ffw // 2
    width = feat * tps
    n = zn * 2
    per = n // tps
    rc = own * 2
    gains = jnp.stack([gain_mixer, gain_mid])
    vmem, hbm = pl.BlockSpec(memory_space=pltpu.VMEM), pl.BlockSpec(memory_space=pl.ANY)
    dma = pltpu.SemaphoreType.DMA
    lanes = tps - 1
    return pl.pallas_call(
        functools.partial(kernel, zn, tps),
        out_shape=jax.ShapeDtypeStruct((rows, feat), bf16),
        in_specs=[vmem] * 4 + [hbm] * 4,
        out_specs=vmem,
        scratch_shapes=[
            pltpu.VMEM((width, cin), bf16),
            pltpu.VMEM((width, cin), bf16),
            pltpu.VMEM((width, fh), bf16),
            pltpu.VMEM((width, fh), bf16),
            pltpu.VMEM((own, ffw), bf16),
            pltpu.VMEM((own, ffw), bf16),
            pltpu.VMEM((tps, rows, feat), bf16),
            pltpu.VMEM((tps, 2, feat), f32),
            pltpu.VMEM((rows, width), bf16),
            pltpu.VMEM((rows, width), bf16),
            pltpu.VMEM((lanes, rows, width), bf16),
            pltpu.VMEM((2, rows, width), bf16),
            pltpu.VMEM((2 * rows, fh), bf16),
            pltpu.VMEM((n, 2 * rows, rc), bf16),
            pltpu.VMEM((lanes, per, 2 * rows, rc), bf16),
            pltpu.VMEM((per, rows, rc), bf16),
            pltpu.VMEM((per, rows, rc), bf16),
            pltpu.VMEM((rows, feat), f32),
            pltpu.VMEM((tps, rows, 128), f32),
            pltpu.VMEM((128, rows), f32),
            pltpu.VMEM((8, rows), f32),
            pltpu.VMEM((lanes, 8, rows), f32),
            pltpu.VMEM((rows, cin), f32),
            dma((6,)),
            dma((5, zn)), dma((5, zn)), dma((5, zn)), dma((5, zn)), dma((5, zn, 2)), dma((5, zn, 2)),
            dma((lanes,)), dma((lanes,)), dma((lanes,)), dma((lanes,)),
            dma((lanes, 2)), dma((lanes, 2)), dma((2,)), dma((2,)), dma((lanes, 2)), dma((lanes, 2)),
            dma((n, 2)), dma((lanes, per, 2)), dma((per,)), dma((per,)), dma((lanes,)), dma((lanes,)),
        ],
        compiler_params=pltpu.CompilerParams(
            collective_id=0, has_side_effects=True, vmem_limit_bytes=67043328
        ),
    )(tokens, gains, pool_scale[None], gain_out[None], w_in, w_pool_out, w_ff1, w_ff2)


def solution(mesh):
    zn, tps = mesh.shape["fs"] // 4, mesh.shape["tp"]
    return jax.shard_map(
        functools.partial(local, zn, tps),
        mesh=mesh,
        in_specs=(
            P("fs", "tp"),
            P("tp"),
            P("fs", "tp"),
            P("tp"),
            P("fs", "tp"),
            P("tp"),
            P("fs", "tp"),
            P("fs", "tp"),
            P("tp"),
        ),
        out_specs=P("fs", "tp"),
        check_vma=False,
    )
```

time: 212 us -> 181 us (0.85)
  Pallas kernels: 207 us -> 175 us
    pallas_call x1, Pallas kernels: 207 us -> 175 us  [local(): pl.pallas_call(functools.partial(kernel, zn, tps), out_shape=jax.ShapeDty...]
where the time goes in v1:
time: 181 us; the launch traced here: 179 us
  Pallas kernels  175 us (97%)
  local copies, waits for them, and re-layouts  2.75 us (2%)
    pallas_call x1, Pallas kernels, local(): pl.pallas_call(functools.partial(kernel, zn, tps), out_shape=jax.ShapeDty...  175 us

profile of v1, /device:TPU:0, one launch (start us, length us, event | category | flops | bytes accessed | tf_op | source)
XLA Modules:
  0.0 178.8 jit_solution(18197405224389691276)
XLA Ops:
  0.0 0.0 copy-start
  0.0 0.7 copy-done
  0.7 1.3 pad_maximum_fusion.gains_ref
  2.0 174.7 %shard_map.91 = bf16[384,1024]{1,0:T(8,128)(2,1)} custom-call(bf16[384,1024]{1,0:T(8,128)(2,1)} %x_ref.1, f32[2,1024]{1,0:T(2,128)} %pad_maximum_fusion.gains_ref, f32[1,512]{1,0:T(1,128)} %bitcast.7, f32[1,1024]{1,0:T(1,128)} %bitcast.6, bf16[128,512]{1,0:T(8,128)(2,1)} %win_ref.1, bf16[128,512]{1,0:T(8,128)(2,1)} %wpo_ref.1, bf16[128,4096]{1,0:T(8,128)(2,1)} %wup_ref.1, ...), custom_call_target="tpu_custom_call" | custom-call | tf_op jit(solution)/shard_map/pallas_call | solution.py:477
  176.7 2.1 %copy.11 = bf16[384,1024]{1,0:T(8,128)(2,1)} copy(bf16[384,1024]{1,0:T(8,128)(2,1)} %shard_map.91) | data formatting | bytes 1572864
Async XLA Ops:
  0.0 0.7 copy-start

commit v2 on v1

--- a/solution.py
+++ b/solution.py
@@ -12,6 +12,7 @@
 residual_alpha = 2.0**0.25
 f32, bf16 = jnp.float32, jnp.bfloat16
 MESH = pl.DeviceIdType.MESH
+scope = jax.named_scope
 
 
 def nt_dot(left, right):
@@ -23,7 +24,7 @@
     x_ref, gains_ref, scale_ref, gout_ref, win_ref, wpo_ref, wup_ref, wdn_ref, out_ref,
     win, wpo, wup, wdn, sup, sdn, xfull, gfull, mixed, mpart, mrecv, middle, hidden,
     part, precv, zpart, zrecv, total, moments, spread, stat, srecv, work,
-    load_sem, zs_sem, zr_sem, ys_sem, yr_sem, ss_sem, sr_sem, xs_sem, xr_sem, gs_sem, gr_sem,
+    load_sem, zs_sem, zq_sem, zr_sem, ys_sem, yr_sem, ss_sem, sr_sem, xs_sem, xr_sem, gs_sem, gr_sem,
     ms_sem, mr_sem, as_sem, ar_sem, fs_sem, fr_sem, rs_sem, rr_sem, ps_sem, pr_sem, ts_sem, tr_sem,
 ):
     i, t = lax.axis_index("fs"), lax.axis_index("tp")
@@ -58,6 +59,7 @@
             if v not in order:
                 order.append(v)
     far = order[1:]
+    near = [1] + [v for j in range(2, zn, 2) for v in (j + 1, j)]
 
     def dev(zz, yy, cc):
         return (zz * 2 + yy) * 2 + cc
@@ -103,23 +105,46 @@
         for j in js:
             zsend(w, j).start()
 
+    def gate(me, other):
+        lower = lax.rem(me, 2) == 0
+        before = lax.div(other, 2) < lax.div(me, 2)
+        return (lower & before) | (~lower & ~before)
+
+    def relay(w, j):
+        b = block(w, across(j), y, c)
+        return remote(b, b, zq_sem.at[w, j], zr_sem.at[w, j ^ 1], mate, t)
+
+    def spread_out(w):
+        zsend(w, 1).start()
+        for j in near[1:]:
+            @pl.when(gate(across(j), z))
+            def _():
+                zsend(w, j).start()
+
     def own_start(w):
         yfwd(w, 0).start()
         share(w, 0, 0).start()
 
     def z_in(w, j):
-        zsend(w, j).wait_recv()
+        with scope(f"z{w}_{j}"):
+            zsend(w, j).wait_recv()
+        if w in (WIN, WPO) and j > 1:
+            @pl.when(gate(z, across(j)))
+            def _():
+                relay(w, j).start()
         yfwd(w, j).start()
         share(w, j, 0).start()
 
     def y_in(w, j):
-        yfwd(w, j).wait_recv()
+        with scope(f"y{w}_{j}"):
+            yfwd(w, j).wait_recv()
         share(w, j, 1).start()
 
     def s_in(w):
-        for j in order:
-            for s in range(2):
-                share(w, j, s).wait_recv()
+        with scope(f"s{w}"):
+            for j in order:
+                for s in range(2):
+                    share(w, j, s).wait_recv()
 
     def x_copy(q):
         return remote(x_ref, xfull.at[t], xs_sem.at[q], xr_sem.at[q], i, peers[q])
@@ -181,20 +206,20 @@
     ]
     for copy in loads:
         copy.start()
-    pl.semaphore_wait(barrier, len(far) + 2 + len(peers))
+    with scope("begin"):
+        pl.semaphore_wait(barrier, len(far) + 2 + len(peers))
 
     for q in range(lanes):
         x_copy(q).start()
         g_copy(q).start()
     loads[0].wait()
     own_start(WIN)
-    zsends(WIN, far)
+    spread_out(WIN)
     loads[1].wait()
     own_start(WPO)
-    zsends(WPO, far)
+    spread_out(WPO)
     loads[2].wait()
     loads[3].wait()
-    zsends(UP0, far)
     xfull[t] = x_ref[...]
     gfull[t] = gains_ref[...]
     loads[4].wait()
@@ -220,33 +245,44 @@
         for r in range(tps):
             mixed[rs, r * feat:(r + 1) * feat] = (pieces[r] * gfull[r, 0:1, :]).astype(bf16)
 
-    zev = [(WIN, j) for j in far] + [(WPO, j) for j in far]
-    yev = [(WIN, 0), (WPO, 0)] + zev
-    for k, ev in enumerate(zev):
-        z_in(*ev)
-        if k >= 1:
-            y_in(*yev[k - 1])
-        if k == len(far):
-            for q in range(lanes):
-                x_copy(q).wait_recv()
-                g_copy(q).wait_recv()
-            blocks_of(first_norm)
+    mids = [j for j in far if j > 1]
+
+    def wave(w, first):
+        for j in mids:
+            ahead = gate(across(j), z)
+
+            @pl.when(ahead if first else ~ahead)
+            def _():
+                zsend(w, j).start()
+
+    for w in (WIN, WPO):
+        for j in near:
+            z_in(w, j)
+    wave(UP0, True)
+    y_in(WIN, 0)
+    y_in(WPO, 0)
+    for j in near[:-1]:
+        y_in(WIN, j)
+    with scope("xwait"):
+        for q in range(lanes):
+            x_copy(q).wait_recv()
+            g_copy(q).wait_recv()
+    with scope("norm1"):
+        blocks_of(first_norm)
+    wave(UP0, False)
+    zsends(UP0, [1])
     own_start(UP0)
-    own_start(UP1)
-    zsends(UP1, far)
-    rest = yev[len(zev) - 1:]
-    for ev in rest:
-        if ev[0] == WIN:
-            y_in(*ev)
-    rest = [ev for ev in rest if ev[0] == WPO]
+    y_in(WIN, near[-1])
+    y_in(WPO, near[0])
     s_in(WIN)
 
     cb = math.gcd(cin, 128)
     gw = cin * tps // 4
-    pool = jnp.dot(mixed[...], win[...], preferred_element_type=f32)
-    work[:, :cin] = pool.astype(bf16).astype(f32)
-    for ev in rest:
-        y_in(*ev)
+    with scope("pooldot"):
+        pool = jnp.dot(mixed[...], win[...], preferred_element_type=f32)
+        work[:, :cin] = pool.astype(bf16).astype(f32)
+    for j in near[1:-1]:
+        y_in(WPO, j)
     row = lax.broadcasted_iota(jnp.int32, (rows, cb), 0)
     position = (row + 1).astype(f32)
     for k in range(cin // cb):
@@ -268,6 +304,8 @@
         count = jnp.minimum(position, pick(2.0, 4.0, 8.0, 16.0))
         mixed[:, cs] = ((pick(s2, s4, s8, s16) / count - u) * scale_ref[0:1, cs]).astype(bf16)
 
+    y_in(WPO, near[-1])
+    own_start(UP1)
     s_in(WPO)
     wb = math.gcd(width, 512)
     for h in range(2):
@@ -276,7 +314,8 @@
             mpart[half(h), cs] = nt_dot(mixed[half(h), :cin], wpo[cs, :]).astype(bf16)
             return carry
 
-        lax.fori_loop(0, width // wb, out_proj, 0)
+        with scope("outproj"):
+            lax.fori_loop(0, width // wb, out_proj, 0)
         for q in range(lanes):
             m_copy(q, h).start()
 
@@ -294,26 +333,33 @@
             middle[role, rs, r * feat:(r + 1) * feat] = (pieces[r] * gfull[r, 1:2, :]).astype(bf16)
 
     def settle(h):
-        for q in range(lanes):
-            m_copy(q, h).wait_recv()
-        blocks_of(second_norm, h * hr, (h + 1) * hr)
+        with scope("mwait"):
+            for q in range(lanes):
+                m_copy(q, h).wait_recv()
+        with scope("norm2"):
+            blocks_of(second_norm, h * hr, (h + 1) * hr)
         a_copy(h).start()
 
-    zev = [(UP0, j) for j in far] + [(UP1, j) for j in far]
-    yev = [(UP0, 0), (UP1, 0)] + zev
-    for k, ev in enumerate(zev):
-        z_in(*ev)
-        y_in(*yev[k])
-        if k == len(far):
-            settle(0)
-        if k == len(far) + 1:
-            own_start(DN)
-            zsends(DN, far[:1])
+    wave(UP1, True)
+    zsends(UP1, [1])
+    z_in(UP0, 1)
+    y_in(UP0, 0)
+    for j in mids:
+        z_in(UP0, j)
+    wave(UP1, False)
+    y_in(UP1, 0)
+    y_in(UP0, 1)
+    settle(0)
+    for j in mids[:-1]:
+        y_in(UP0, j)
+    zsends(DN, mids[:1])
+    z_in(UP1, 1)
+    y_in(UP0, mids[-1])
+    for j in mids:
+        z_in(UP1, j)
+    own_start(DN)
     settle(1)
-    zsends(DN, far[1:])
-    for ev in yev[len(zev):]:
-        y_in(*ev)
-
+    zsends(DN, [1])
     hb = math.gcd(fq, 512)
 
     def ff1(s, lo, hi):
@@ -322,36 +368,62 @@
             act = jnp.maximum(jnp.dot(middle[s], wup[:, cs], preferred_element_type=f32), 0.0)
             hidden[slot(s), cs] = (act * act).astype(bf16)
             return carry
-        lax.fori_loop(0, (hi - lo) // hb, up, 0)
+        with scope("ff1"):
+            lax.fori_loop(0, (hi - lo) // hb, up, 0)
 
     def pass_on(h):
         a_back = middle.at[1 - role, half(h), slab]
-        remote(a_back, a_back, as_sem.at[h], ar_sem.at[h], mate, t).wait_recv()
+        with scope("await"):
+            remote(a_back, a_back, as_sem.at[h], ar_sem.at[h], mate, t).wait_recv()
         for q in range(lanes):
             f_copy(q, h).start()
 
+    y_in(UP1, 1)
+    pass_on(0)
+    for j in mids[:-1]:
+        y_in(UP1, j)
     s_in(UP0)
     ff1(role, 0, fq)
-    pass_on(0)
-    z_in(DN, far[0])
+    y_in(UP1, mids[-1])
     s_in(UP1)
     ff1(role, fq, fh)
+    zsends(DN, mids[1:])
     pass_on(1)
-    y_in(DN, 0)
-    for h in range(2):
-        for q in range(lanes):
-            f_copy(q, h).wait_recv()
-    ff1(1 - role, 0, fh)
-
-    def down(j, s):
-        g = across(j) * 2 + (y if s == 0 else 1 - y)
-        share(DN, j, s).wait_recv()
-        part[g] = nt_dot(hidden[...], wdn[pl.ds(pl.multiple_of(g * rc, rc), rc), :]).astype(bf16)
+
+    def group(j, s):
+        return across(j) * 2 + (y if s == 0 else 1 - y)
+
+    landed = []
+
+    def down(j, s, kept):
+        g = group(j, s)
+        which = role if kept else 1 - role
+        if (j, s) not in landed:
+            landed.append((j, s))
+            with scope(f"dshare{j}_{s}"):
+                share(DN, j, s).wait_recv()
+        with scope("ff2"):
+            w = wdn[pl.ds(pl.multiple_of(g * rc, rc), rc), :]
+            part[g, slot(which), :] = nt_dot(hidden[slot(which), :], w).astype(bf16)
 
         @pl.when(lax.div(g, per) != t)
         def _():
-            r_copy(g, 0).start()
-            r_copy(g, 1).start()
+            r_copy(g, 1 if kept else 0).start()
+
+    down(0, 0, True)
+    y_in(DN, 0)
+    z_in(DN, far[0])
+    down(0, 1, True)
+    down(far[0], 0, True)
+    with scope("fwait"):
+        for h in range(2):
+            for q in range(lanes):
+                f_copy(q, h).wait_recv()
+    ff1(1 - role, 0, fh)
+    for ev in ((0, 0), (0, 1), (far[0], 0)):
+        down(*ev, False)
+    z_in(DN, far[1])
+    y_in(DN, far[0])
 
     def fold(j, s):
         g = across(j) * 2 + (y if s == 0 else 1 - y)
@@ -359,31 +431,43 @@
 
         @pl.when(lax.div(g, per) == t)
         def _():
-            for q in range(lanes):
-                r_wait(q, gl, 0)
+            with scope(f"rwait{j}_{s}"):
+                for q in range(lanes):
+                    r_wait(q, gl, 0)
             v = part[g, slot(1 - role), :].astype(f32)
             for q in range(lanes):
                 v = v + precv[q, gl, slot(1 - role), :].astype(f32)
             zpart[gl] = v.astype(bf16)
             p_copy(gl).start()
 
-    for k, j in enumerate(order):
-        if k + 2 < zn:
-            z_in(DN, order[k + 2])
-        down(j, 0)
-        if k + 1 < zn:
-            y_in(DN, order[k + 1])
-        down(j, 1)
-        if k:
-            for s in range(2):
-                fold(order[k - 1], s)
-    for s in range(2):
-        fold(order[-1], s)
+    def both(j, s):
+        down(j, s, False)
+        down(j, s, True)
+
+    both(far[0], 1)
+    both(far[1], 0)
+    pending = [(0, 0), (0, 1), (far[0], 0), (far[0], 1), (far[1], 0)]
+    for k in range(1, len(far)):
+        if k + 1 < len(far):
+            z_in(DN, far[k + 1])
+        for ev in pending[:2]:
+            fold(*ev)
+        pending = pending[2:]
+        y_in(DN, far[k])
+        both(far[k], 1)
+        pending.append((far[k], 1))
+        if k + 1 < len(far):
+            both(far[k + 1], 0)
+            pending.append((far[k + 1], 0))
+    for ev in pending:
+        fold(*ev)
 
     for gl in range(per):
-        for q in range(lanes):
-            r_wait(q, gl, 1)
-        p_copy(gl).wait_recv()
+        with scope(f"r1wait{gl}"):
+            for q in range(lanes):
+                r_wait(q, gl, 1)
+        with scope(f"pwait{gl}"):
+            p_copy(gl).wait_recv()
 
     lane = lax.broadcasted_iota(jnp.int32, (rb, 128), 1)
 
@@ -407,13 +491,15 @@
             square = square + jnp.sum((v - mean) * (v - mean), axis=1, keepdims=True)
         moments[0, rs, :] = jnp.where(lane == 0, mean, jnp.where(lane == 1, square, 0.0))
 
-    blocks_of(gather_up)
+    with scope("gather_up"):
+        blocks_of(gather_up)
     stat[...] = jnp.transpose(moments[0])[0:8, :]
     for q in range(lanes):
         t_copy(q).start()
     spread[...] = jnp.zeros_like(spread)
     for q in range(lanes):
-        t_copy(q).wait_recv()
+        with scope("twait"):
+            t_copy(q).wait_recv()
         spread[0:8, :] = srecv[q]
         moments[q + 1] = jnp.transpose(spread[...])
 
@@ -426,7 +512,8 @@
         inv = lax.rsqrt(square / width + norm_eps)
         out_ref[rs, :] = ((total[rs, :] - mean) * inv * gout_ref[0:1, :]).astype(bf16)
 
-    blocks_of(last_norm)
+    with scope("norm3"):
+        blocks_of(last_norm)
 
     for q in range(lanes):
         x_copy(q).wait_send()
@@ -454,8 +541,16 @@
     lax.fori_loop(0, per, folded, 0)
     for w in range(len(streams)):
         for j in order:
-            if j:
+            if j == 1 or (j and w not in (WIN, WPO)):
                 zsend(w, j).wait_send()
+            elif j:
+                @pl.when(gate(across(j), z))
+                def _():
+                    zsend(w, j).wait_send()
+
+                @pl.when(gate(z, across(j)))
+                def _():
+                    relay(w, j).wait_send()
             yfwd(w, j).wait_send()
             share(w, j, 0).wait_send()
             share(w, j, 1).wait_send()
@@ -504,7 +599,7 @@
             pltpu.VMEM((lanes, 8, rows), f32),
             pltpu.VMEM((rows, cin), f32),
             dma((6,)),
-            dma((5, zn)), dma((5, zn)), dma((5, zn)), dma((5, zn)), dma((5, zn, 2)), dma((5, zn, 2)),
+            dma((5, zn)), dma((2, zn)), dma((5, zn)), dma((5, zn)), dma((5, zn)), dma((5, zn, 2)), dma((5, zn, 2)),
             dma((lanes,)), dma((lanes,)), dma((lanes,)), dma((lanes,)),
             dma((lanes, 2)), dma((lanes, 2)), dma((2,)), dma((2,)), dma((lanes, 2)), dma((lanes, 2)),
             dma((n, 2)), dma((lanes, per, 2)), dma((per,)), dma((per,)), dma((lanes,)), dma((lanes,)),

time: 181 us -> 169 us (0.934); the launches traced: 179 us -> 169 us
  Pallas kernels: 175 us -> 165 us
    pallas_call x1, Pallas kernels: 175 us -> 165 us  [local(): pl.pallas_call(functools.partial(kernel, zn, tps), out_shape=jax.ShapeDty...]
where the time goes in v2:
time: 169 us
  Pallas kernels  165 us (98%)
  local copies, waits for them, and re-layouts  2.75 us (2%)
    pallas_call x1, Pallas kernels, local(): pl.pallas_call(functools.partial(kernel, zn, tps), out_shape=jax.ShapeDty...  165 us

profile of v2, /device:TPU:0, one launch (start us, length us, event | category | flops | bytes accessed | tf_op | source)
XLA Modules:
  0.0 168.8 jit_solution(909050351824746808)
XLA Ops:
  0.0 0.0 copy-start
  0.0 0.7 copy-done
  0.7 1.3 pad_maximum_fusion.gains_ref
  2.0 164.8 %shard_map.91 = bf16[384,1024]{1,0:T(8,128)(2,1)} custom-call(bf16[384,1024]{1,0:T(8,128)(2,1)} %x_ref.1, f32[2,1024]{1,0:T(2,128)} %pad_maximum_fusion.gains_ref, f32[1,512]{1,0:T(1,128)} %bitcast.7, f32[1,1024]{1,0:T(1,128)} %bitcast.6, bf16[128,512]{1,0:T(8,128)(2,1)} %win_ref.1, bf16[128,512]{1,0:T(8,128)(2,1)} %wpo_ref.1, bf16[128,4096]{1,0:T(8,128)(2,1)} %wup_ref.1, ...), custom_call_target="tpu_custom_call" | custom-call | tf_op jit(solution)/shard_map/pallas_call | solution.py:572
  166.8 2.1 %copy.11 = bf16[384,1024]{1,0:T(8,128)(2,1)} copy(bf16[384,1024]{1,0:T(8,128)(2,1)} %shard_map.91) | data formatting | bytes 1572864
Async XLA Ops:
  0.0 0.7 copy-start

commit v3 on v2

--- a/solution.py
+++ b/solution.py
@@ -21,7 +21,7 @@
 
 def kernel(
     zn, tps,
-    x_ref, gains_ref, scale_ref, gout_ref, win_ref, wpo_ref, wup_ref, wdn_ref, out_ref,
+    x_ref, ga_ref, gb_ref, scale_ref, gout_ref, win_ref, wpo_ref, wup_ref, wdn_ref, out_ref,
     win, wpo, wup, wdn, sup, sdn, xfull, gfull, mixed, mpart, mrecv, middle, hidden,
     part, precv, zpart, zrecv, total, moments, spread, stat, srecv, work,
     load_sem, zs_sem, zq_sem, zr_sem, ys_sem, yr_sem, ss_sem, sr_sem, xs_sem, xr_sem, gs_sem, gr_sem,
@@ -42,7 +42,8 @@
     n = zn * 2
     per = n // tps
     rc = own * 2
-    hr = rows // 2
+    cut = rows // 2
+    ends = (0, cut, rows)
     lanes = tps - 1
 
     def across(j):
@@ -147,13 +148,13 @@
                     share(w, j, s).wait_recv()
 
     def x_copy(q):
-        return remote(x_ref, xfull.at[t], xs_sem.at[q], xr_sem.at[q], i, peers[q])
-
-    def g_copy(q):
-        return remote(gains_ref, gfull.at[t], gs_sem.at[q], gr_sem.at[q], i, peers[q])
+        return remote(xfull.at[t], xfull.at[t], xs_sem.at[q], xr_sem.at[q], i, peers[q])
+
+    def g_copy(q, k):
+        return remote((ga_ref, gb_ref)[k], gfull.at[k, t], gs_sem.at[q, k], gr_sem.at[q, k], i, peers[q])
 
     def half(h):
-        return pl.ds(h * hr, hr)
+        return pl.ds(ends[h], ends[h + 1] - ends[h])
 
     def m_copy(q, h):
         return remote(mpart.at[half(h)], mrecv.at[q, half(h)], ms_sem.at[q, h], mr_sem.at[q, h], i, peers[q])
@@ -204,14 +205,18 @@
         pltpu.make_async_copy(wdn_ref, sdn, load_sem.at[4]),
         pltpu.make_async_copy(wdn_ref.at[:, part_cols], wdn.at[mine], load_sem.at[5]),
     ]
+    x_load = pltpu.make_async_copy(x_ref, xfull.at[t], load_sem.at[6])
+    x_load.start()
     for copy in loads:
         copy.start()
     with scope("begin"):
         pl.semaphore_wait(barrier, len(far) + 2 + len(peers))
 
+    x_load.wait()
     for q in range(lanes):
         x_copy(q).start()
-        g_copy(q).start()
+        for k in range(2):
+            g_copy(q, k).start()
     loads[0].wait()
     own_start(WIN)
     spread_out(WIN)
@@ -220,18 +225,18 @@
     spread_out(WPO)
     loads[2].wait()
     loads[3].wait()
-    xfull[t] = x_ref[...]
-    gfull[t] = gains_ref[...]
+    gfull[0, t] = ga_ref[...]
+    gfull[1, t] = gb_ref[...]
     loads[4].wait()
     loads[5].wait()
 
-    rb = math.gcd(hr, 32)
+    rb = math.gcd(math.gcd(cut, rows - cut), 32)
 
     def blocks_of(body, lo=0, hi=rows):
         def step(r, carry):
             body(pl.ds(pl.multiple_of(lo + r * rb, rb), rb))
             return carry
-        lax.fori_loop(0, (hi - lo) // rb, step, 0)
+        lax.fori_loop(0, (hi - lo) // rb, step, 0, unroll=2)
 
     def norm(pieces):
         mean = sum(jnp.sum(v, axis=1, keepdims=True) for v in pieces) / width
@@ -243,7 +248,7 @@
     def first_norm(rs):
         pieces = norm([xfull[r, rs, :].astype(f32) for r in range(tps)])
         for r in range(tps):
-            mixed[rs, r * feat:(r + 1) * feat] = (pieces[r] * gfull[r, 0:1, :]).astype(bf16)
+            mixed[rs, r * feat:(r + 1) * feat] = (pieces[r] * gfull[0, r]).astype(bf16)
 
     mids = [j for j in far if j > 1]
 
@@ -255,9 +260,22 @@
             def _():
                 zsend(w, j).start()
 
-    for w in (WIN, WPO):
-        for j in near:
-            z_in(w, j)
+    edge = (z == 0) | (z == zn - 1)
+    z_in(WIN, 1)
+
+    @pl.when(edge)
+    def _():
+        z_in(WPO, 1)
+
+    for j in near[1:]:
+        z_in(WIN, j)
+
+    @pl.when(~edge)
+    def _():
+        z_in(WPO, 1)
+
+    for j in near[1:]:
+        z_in(WPO, j)
     wave(UP0, True)
     y_in(WIN, 0)
     y_in(WPO, 0)
@@ -266,7 +284,8 @@
     with scope("xwait"):
         for q in range(lanes):
             x_copy(q).wait_recv()
-            g_copy(q).wait_recv()
+            for k in range(2):
+                g_copy(q, k).wait_recv()
     with scope("norm1"):
         blocks_of(first_norm)
     wave(UP0, False)
@@ -330,14 +349,14 @@
             pieces.append(residual_alpha * xfull[r, rs, :].astype(f32) + mix)
         pieces = norm(pieces)
         for r in range(tps):
-            middle[role, rs, r * feat:(r + 1) * feat] = (pieces[r] * gfull[r, 1:2, :]).astype(bf16)
+            middle[role, rs, r * feat:(r + 1) * feat] = (pieces[r] * gfull[1, r]).astype(bf16)
 
     def settle(h):
         with scope("mwait"):
             for q in range(lanes):
                 m_copy(q, h).wait_recv()
         with scope("norm2"):
-            blocks_of(second_norm, h * hr, (h + 1) * hr)
+            blocks_of(second_norm, ends[h], ends[h + 1])
         a_copy(h).start()
 
     wave(UP1, True)
@@ -352,14 +371,19 @@
     settle(0)
     for j in mids[:-1]:
         y_in(UP0, j)
-    zsends(DN, mids[:1])
     z_in(UP1, 1)
     y_in(UP0, mids[-1])
     for j in mids:
         z_in(UP1, j)
     own_start(DN)
+    y_in(UP1, 1)
+    zsends(DN, mids[:1])
     settle(1)
-    zsends(DN, [1])
+
+    @pl.when(edge)
+    def _():
+        zsends(DN, [1])
+
     hb = math.gcd(fq, 512)
 
     def ff1(s, lo, hi):
@@ -378,7 +402,6 @@
         for q in range(lanes):
             f_copy(q, h).start()
 
-    y_in(UP1, 1)
     pass_on(0)
     for j in mids[:-1]:
         y_in(UP1, j)
@@ -387,15 +410,13 @@
     y_in(UP1, mids[-1])
     s_in(UP1)
     ff1(role, fq, fh)
-    zsends(DN, mids[1:])
-    pass_on(1)
 
     def group(j, s):
         return across(j) * 2 + (y if s == 0 else 1 - y)
 
     landed = []
 
-    def down(j, s, kept):
+    def down(j, s, kept, start=True):
         g = group(j, s)
         which = role if kept else 1 - role
         if (j, s) not in landed:
@@ -406,27 +427,22 @@
             w = wdn[pl.ds(pl.multiple_of(g * rc, rc), rc), :]
             part[g, slot(which), :] = nt_dot(hidden[slot(which), :], w).astype(bf16)
 
+        if start:
+            hand(j, s, kept)
+
+    def hand(j, s, kept):
+        g = group(j, s)
+
         @pl.when(lax.div(g, per) != t)
         def _():
             r_copy(g, 1 if kept else 0).start()
 
-    down(0, 0, True)
-    y_in(DN, 0)
-    z_in(DN, far[0])
-    down(0, 1, True)
-    down(far[0], 0, True)
-    with scope("fwait"):
-        for h in range(2):
-            for q in range(lanes):
-                f_copy(q, h).wait_recv()
-    ff1(1 - role, 0, fh)
-    for ev in ((0, 0), (0, 1), (far[0], 0)):
-        down(*ev, False)
-    z_in(DN, far[1])
-    y_in(DN, far[0])
+    def both(j, s):
+        down(j, s, False)
+        down(j, s, True)
 
     def fold(j, s):
-        g = across(j) * 2 + (y if s == 0 else 1 - y)
+        g = group(j, s)
         gl = lax.rem(g, per)
 
         @pl.when(lax.div(g, per) == t)
@@ -440,62 +456,138 @@
             zpart[gl] = v.astype(bf16)
             p_copy(gl).start()
 
-    def both(j, s):
-        down(j, s, False)
-        down(j, s, True)
-
-    both(far[0], 1)
-    both(far[1], 0)
-    pending = [(0, 0), (0, 1), (far[0], 0), (far[0], 1), (far[1], 0)]
-    for k in range(1, len(far)):
-        if k + 1 < len(far):
+    def residual(rs):
+        base = middle[role, rs, slab]
+        for gl in range(per):
+            total[gl, rs, :] = residual_alpha * base[:, gl * rc:(gl + 1) * rc].astype(f32)
+
+    def prep(j, s):
+        g = group(j, s)
+        gl = lax.rem(g, per)
+
+        @pl.when(lax.div(g, per) == t)
+        def _():
+            with scope(f"pwait{j}_{s}"):
+                for q in range(lanes):
+                    r_wait(q, gl, 1)
+                p_copy(gl).wait_recv()
+            with scope("prep"):
+                ff = part[g, slot(role), :].astype(f32)
+                for q in range(lanes):
+                    ff = ff + precv[q, gl, slot(role), :].astype(f32)
+                total[gl] = total[gl] + (ff + zrecv[gl].astype(f32)).astype(bf16).astype(f32)
+
+    down(0, 0, True)
+    pass_on(1)
+
+    @pl.when(~edge)
+    def _():
+        zsends(DN, [1])
+        zsends(DN, mids[1:])
+
+    z_in(DN, far[0])
+    down(far[0], 0, True, False)
+    blocks_of(residual)
+    y_in(DN, 0)
+    down(0, 1, True, False)
+
+    @pl.when(~edge)
+    def _():
+        z_in(DN, 1)
+
+    with scope("fwait"):
+        for h in range(2):
+            for q in range(lanes):
+                f_copy(q, h).wait_recv()
+
+    @pl.when(edge)
+    def _():
+        zsends(DN, mids[1:])
+        z_in(DN, 1)
+
+    ff1(1 - role, 0, fh)
+    for ev in ((0, 0), (far[0], 0), (0, 1)):
+        down(*ev, False)
+    for ev in ((far[0], 0), (0, 1)):
+        hand(*ev, True)
+    pending = [(0, 0), (far[0], 0), (0, 1)]
+    done = []
+    for k in range(len(far)):
+        if k and k + 1 < len(far):
             z_in(DN, far[k + 1])
-        for ev in pending[:2]:
-            fold(*ev)
-        pending = pending[2:]
         y_in(DN, far[k])
         both(far[k], 1)
         pending.append((far[k], 1))
         if k + 1 < len(far):
             both(far[k + 1], 0)
             pending.append((far[k + 1], 0))
+            for ev in pending[:2 + k]:
+                fold(*ev)
+            done += pending[:2 + k]
+            pending = pending[2 + k:]
     for ev in pending:
         fold(*ev)
-
-    for gl in range(per):
-        with scope(f"r1wait{gl}"):
-            for q in range(lanes):
-                r_wait(q, gl, 1)
-        with scope(f"pwait{gl}"):
-            p_copy(gl).wait_recv()
+    for ev in done + pending:
+        prep(*ev)
 
     lane = lax.broadcasted_iota(jnp.int32, (rb, 128), 1)
 
     def gather_up(rs):
-        own_rows = pl.ds(pl.multiple_of(role * rows + rs.start, rb), rb)
-        base = middle[role, rs, slab]
-        values = []
-        mean = jnp.zeros((rb, 1), f32)
+        mean = sum(jnp.sum(total[gl, rs, :], axis=1, keepdims=True) for gl in range(per)) / feat
+        square = jnp.zeros((rb, 1), f32)
         for gl in range(per):
-            ff = part[t * per + gl, own_rows, :].astype(f32)
-            for q in range(lanes):
-                ff = ff + precv[q, gl, own_rows, :].astype(f32)
-            ff = (ff + zrecv[gl, rs, :].astype(f32)).astype(bf16).astype(f32)
-            v = residual_alpha * base[:, gl * rc:(gl + 1) * rc].astype(f32) + ff
-            total[rs, gl * rc:(gl + 1) * rc] = v
-            values.append(v)
-            mean = mean + jnp.sum(v, axis=1, keepdims=True)
-        mean = mean / feat
-        square = jnp.zeros((rb, 1), f32)
-        for v in values:
-            square = square + jnp.sum((v - mean) * (v - mean), axis=1, keepdims=True)
+            v = total[gl, rs, :] - mean
+            square = square + jnp.sum(v * v, axis=1, keepdims=True)
         moments[0, rs, :] = jnp.where(lane == 0, mean, jnp.where(lane == 1, square, 0.0))
 
     with scope("gather_up"):
         blocks_of(gather_up)
+
+    def drain():
+        for q in range(lanes):
+            x_copy(q).wait_send()
+            for k in range(2):
+                g_copy(q, k).wait_send()
+            for h in range(2):
+                m_copy(q, h).wait_send()
+                f_copy(q, h).wait_send()
+        for h in range(2):
+            a_copy(h).wait_send()
+
+        def sent(g, carry):
+            @pl.when(lax.div(g, per) != t)
+            def _():
+                r_copy(g, 0).wait_send()
+                r_copy(g, 1).wait_send()
+            return carry
+
+        lax.fori_loop(0, n, sent, 0)
+
+        def folded(gl, carry):
+            p_copy(gl).wait_send()
+            return carry
+
+        lax.fori_loop(0, per, folded, 0)
+        for w in range(len(streams)):
+            for j in order:
+                if j == 1 or (j and w not in (WIN, WPO)):
+                    zsend(w, j).wait_send()
+                elif j:
+                    @pl.when(gate(across(j), z))
+                    def _():
+                        zsend(w, j).wait_send()
+
+                    @pl.when(gate(z, across(j)))
+                    def _():
+                        relay(w, j).wait_send()
+                yfwd(w, j).wait_send()
+                share(w, j, 0).wait_send()
+                share(w, j, 1).wait_send()
+
     stat[...] = jnp.transpose(moments[0])[0:8, :]
     for q in range(lanes):
         t_copy(q).start()
+    drain()
     spread[...] = jnp.zeros_like(spread)
     for q in range(lanes):
         with scope("twait"):
@@ -510,50 +602,15 @@
         for m in means:
             square = square + feat * (m - mean) * (m - mean)
         inv = lax.rsqrt(square / width + norm_eps)
-        out_ref[rs, :] = ((total[rs, :] - mean) * inv * gout_ref[0:1, :]).astype(bf16)
+        for gl in range(per):
+            cs = slice(gl * rc, (gl + 1) * rc)
+            out_ref[rs, cs] = ((total[gl, rs, :] - mean) * inv * gout_ref[0:1, cs]).astype(bf16)
 
     with scope("norm3"):
         blocks_of(last_norm)
 
     for q in range(lanes):
-        x_copy(q).wait_send()
-        g_copy(q).wait_send()
         t_copy(q).wait_send()
-        for h in range(2):
-            m_copy(q, h).wait_send()
-            f_copy(q, h).wait_send()
-    for h in range(2):
-        a_copy(h).wait_send()
-
-    def sent(g, carry):
-        @pl.when(lax.div(g, per) != t)
-        def _():
-            r_copy(g, 0).wait_send()
-            r_copy(g, 1).wait_send()
-        return carry
-
-    lax.fori_loop(0, n, sent, 0)
-
-    def folded(gl, carry):
-        p_copy(gl).wait_send()
-        return carry
-
-    lax.fori_loop(0, per, folded, 0)
-    for w in range(len(streams)):
-        for j in order:
-            if j == 1 or (j and w not in (WIN, WPO)):
-                zsend(w, j).wait_send()
-            elif j:
-                @pl.when(gate(across(j), z))
-                def _():
-                    zsend(w, j).wait_send()
-
-                @pl.when(gate(z, across(j)))
-                def _():
-                    relay(w, j).wait_send()
-            yfwd(w, j).wait_send()
-            share(w, j, 0).wait_send()
-            share(w, j, 1).wait_send()
 
 
 def local(zn, tps, tokens, gain_mixer, w_in, pool_scale, w_pool_out, gain_mid, w_ff1, w_ff2, gain_out):
@@ -565,14 +622,13 @@
     n = zn * 2
     per = n // tps
     rc = own * 2
-    gains = jnp.stack([gain_mixer, gain_mid])
     vmem, hbm = pl.BlockSpec(memory_space=pltpu.VMEM), pl.BlockSpec(memory_space=pl.ANY)
     dma = pltpu.SemaphoreType.DMA
     lanes = tps - 1
     return pl.pallas_call(
         functools.partial(kernel, zn, tps),
         out_shape=jax.ShapeDtypeStruct((rows, feat), bf16),
-        in_specs=[vmem] * 4 + [hbm] * 4,
+        in_specs=[hbm] + [vmem] * 4 + [hbm] * 4,
         out_specs=vmem,
         scratch_shapes=[
             pltpu.VMEM((width, cin), bf16),
@@ -582,7 +638,7 @@
             pltpu.VMEM((own, ffw), bf16),
             pltpu.VMEM((own, ffw), bf16),
             pltpu.VMEM((tps, rows, feat), bf16),
-            pltpu.VMEM((tps, 2, feat), f32),
+            pltpu.VMEM((2, tps, 1, feat), f32),
             pltpu.VMEM((rows, width), bf16),
             pltpu.VMEM((rows, width), bf16),
             pltpu.VMEM((lanes, rows, width), bf16),
@@ -592,22 +648,22 @@
             pltpu.VMEM((lanes, per, 2 * rows, rc), bf16),
             pltpu.VMEM((per, rows, rc), bf16),
             pltpu.VMEM((per, rows, rc), bf16),
-            pltpu.VMEM((rows, feat), f32),
+            pltpu.VMEM((per, rows, rc), f32),
             pltpu.VMEM((tps, rows, 128), f32),
             pltpu.VMEM((128, rows), f32),
             pltpu.VMEM((8, rows), f32),
             pltpu.VMEM((lanes, 8, rows), f32),
             pltpu.VMEM((rows, cin), f32),
-            dma((6,)),
+            dma((7,)),
             dma((5, zn)), dma((2, zn)), dma((5, zn)), dma((5, zn)), dma((5, zn)), dma((5, zn, 2)), dma((5, zn, 2)),
-            dma((lanes,)), dma((lanes,)), dma((lanes,)), dma((lanes,)),
+            dma((lanes,)), dma((lanes,)), dma((lanes, 2)), dma((lanes, 2)),
             dma((lanes, 2)), dma((lanes, 2)), dma((2,)), dma((2,)), dma((lanes, 2)), dma((lanes, 2)),
             dma((n, 2)), dma((lanes, per, 2)), dma((per,)), dma((per,)), dma((lanes,)), dma((lanes,)),
         ],
         compiler_params=pltpu.CompilerParams(
             collective_id=0, has_side_effects=True, vmem_limit_bytes=67043328
         ),
-    )(tokens, gains, pool_scale[None], gain_out[None], w_in, w_pool_out, w_ff1, w_ff2)
+    )(tokens, gain_mixer[None], gain_mid[None], pool_scale[None], gain_out[None], w_in, w_pool_out, w_ff1, w_ff2)
 
 
 def solution(mesh):

time: 169 us -> 156 us (0.923)
  Pallas kernels: 165 us -> 154 us
    pallas_call x1, Pallas kernels: 165 us -> 154 us  [local(): pl.pallas_call(functools.partial(kernel, zn, tps), out_shape=jax.ShapeDty...]
where the time goes in v3:
time: 156 us
  Pallas kernels  154 us (99%)
  local copies, waits for them, and re-layouts  2.06 us (1%)
    pallas_call x1, Pallas kernels, local(): pl.pallas_call(functools.partial(kernel, zn, tps), out_shape=jax.ShapeDty...  154 us

profile of v3, /device:TPU:0, one launch (start us, length us, event | category | flops | bytes accessed | tf_op | source)
XLA Modules:
  0.0 155.8 jit_solution(2218410050423925750)
XLA Ops:
  0.0 153.7 %shard_map.91 = bf16[384,1024]{1,0:T(8,128)(2,1)} custom-call(bf16[384,1024]{1,0:T(8,128)(2,1)} %x_ref.1, f32[1,1024]{1,0:T(1,128)} %bitcast.4, f32[1,1024]{1,0:T(1,128)} %bitcast.5, f32[1,512]{1,0:T(1,128)} %bitcast.7, f32[1,1024]{1,0:T(1,128)} %bitcast.6, bf16[128,512]{1,0:T(8,128)(2,1)} %win_ref.1, bf16[128,512]{1,0:T(8,128)(2,1)} %wpo_ref.1, ...), custom_call_target="tpu_custom_call" | custom-call | tf_op jit(solution)/shard_map/pallas_call | solution.py:628
  153.7 2.1 %copy.11 = bf16[384,1024]{1,0:T(8,128)(2,1)} copy(bf16[384,1024]{1,0:T(8,128)(2,1)} %shard_map.91) | data formatting | bytes 1572864

commit v4 on v3

--- a/solution.py
+++ b/solution.py
@@ -37,8 +37,9 @@
     width = feat * tps
     own = win_ref.shape[0]
     ffw = wup_ref.shape[1]
-    fh = ffw // 2
-    fq = fh // 2
+    spare = ffw // 16 // 256 * 256
+    fh = (ffw - spare) // 2
+    fq = -(-fh // 256) * 128
     n = zn * 2
     per = n // tps
     rc = own * 2
@@ -62,6 +63,13 @@
     far = order[1:]
     near = [1] + [v for j in range(2, zn, 2) for v in (j + 1, j)]
 
+    def central(zz):
+        low = lax.div(zz, max(zn // 2, 1)) == 0
+        odd = lax.rem(zz, 2) == 1
+        return (low & odd) | (~low & ~odd)
+
+    taker = central(z)
+
     def dev(zz, yy, cc):
         return (zz * 2 + yy) * 2 + cc
 
@@ -71,8 +79,12 @@
     peers = [lax.rem(t + q, tps) for q in range(1, tps)]
     mine = pl.ds(pl.multiple_of(i * own, own), own)
 
-    WIN, WPO, UP0, UP1, DN = range(5)
-    streams = [(win, 0, cin), (wpo, 0, cin), (wup, 0, fq), (wup, fq, fq), (wdn, 0, fh)]
+    WIN, WPO, UP0, UPA, DN0, DNA, UPX, DNX = range(8)
+    extra = (UPX, DNX)
+    UP1 = (UPA, UPX) if spare else UPA
+    DN = (DN0, DNA, DNX) if spare else (DN0, DNA)
+    streams = [(win, 0, cin), (wpo, 0, cin), (wup, 0, fq), (wup, fq, fh - fq),
+               (wdn, 0, fq), (wdn, fq, fh - fq), (wup, fh, spare), (wdn, fh, spare)]
 
     def block(w, zz, yy, cc):
         ref, c0, cw = streams[w]
@@ -90,8 +102,9 @@
         if w in (WIN, WPO):
             src = b
         else:
-            stage = sdn if w == DN else sup
-            src = stage.at[:, pl.ds(pl.multiple_of(lax.rem(zd, 2) * fh + c0, 128), cw)]
+            stage = sdn if ref is wdn else sup
+            first = 2 * fh if w in extra else lax.rem(zd, 2) * fh + c0
+            src = stage.at[:, pl.ds(pl.multiple_of(first, 128), cw)]
         return remote(src, b, zs_sem.at[w, j], zr_sem.at[w, j], dev(zd, y, c), t)
 
     def yfwd(w, j):
@@ -102,9 +115,22 @@
         b = block(w, across(j), y if s == 0 else 1 - y, c)
         return remote(b, b, ss_sem.at[w, j, s], sr_sem.at[w, j, s], sib, t)
 
-    def zsends(w, js):
+    def parts(w):
+        return w if isinstance(w, tuple) else (w,)
+
+    def having(w, cond, act):
+        if w in extra:
+            pl.when(cond)(act)
+        else:
+            act()
+
+    def zpush(ws, j):
+        for w in parts(ws):
+            having(w, central(across(j)), lambda: zsend(w, j).start())
+
+    def zsends(ws, js):
         for j in js:
-            zsend(w, j).start()
+            zpush(ws, j)
 
     def gate(me, other):
         lower = lax.rem(me, 2) == 0
@@ -122,33 +148,49 @@
             def _():
                 zsend(w, j).start()
 
-    def own_start(w):
-        yfwd(w, 0).start()
-        share(w, 0, 0).start()
-
-    def z_in(w, j):
-        with scope(f"z{w}_{j}"):
-            zsend(w, j).wait_recv()
-        if w in (WIN, WPO) and j > 1:
-            @pl.when(gate(z, across(j)))
-            def _():
-                relay(w, j).start()
-        yfwd(w, j).start()
-        share(w, j, 0).start()
-
-    def y_in(w, j):
-        with scope(f"y{w}_{j}"):
-            yfwd(w, j).wait_recv()
-        share(w, j, 1).start()
-
-    def s_in(w):
-        with scope(f"s{w}"):
+    def own_start(ws):
+        for w in parts(ws):
+            def act():
+                yfwd(w, 0).start()
+                share(w, 0, 0).start()
+            having(w, taker, act)
+
+    def z_in(ws, j):
+        for w in parts(ws):
+            def act():
+                with scope(f"z{w}_{j}"):
+                    zsend(w, j).wait_recv()
+                if w in (WIN, WPO) and j > 1:
+                    @pl.when(gate(z, across(j)))
+                    def _():
+                        relay(w, j).start()
+                yfwd(w, j).start()
+                share(w, j, 0).start()
+            having(w, taker, act)
+
+    def y_in(ws, j):
+        for w in parts(ws):
+            def act():
+                with scope(f"y{w}_{j}"):
+                    yfwd(w, j).wait_recv()
+                share(w, j, 1).start()
+            having(w, taker, act)
+
+    def s_wait(ws, j, s):
+        for w in parts(ws):
+            having(w, taker, lambda: share(w, j, s).wait_recv())
+
+    def s_in(ws):
+        with scope(f"s{parts(ws)[0]}"):
             for j in order:
                 for s in range(2):
-                    share(w, j, s).wait_recv()
-
-    def x_copy(q):
-        return remote(xfull.at[t], xfull.at[t], xs_sem.at[q], xr_sem.at[q], i, peers[q])
+                    s_wait(ws, j, s)
+
+    head = rows * 3 // 4
+
+    def x_copy(q, k):
+        b = xfull.at[t, pl.ds(k * head, (rows - head) if k else head)]
+        return remote(b, b, xs_sem.at[q, k], xr_sem.at[q, k], i, peers[q])
 
     def g_copy(q, k):
         return remote((ga_ref, gb_ref)[k], gfull.at[k, t], gs_sem.at[q, k], gr_sem.at[q, k], i, peers[q])
@@ -201,10 +243,14 @@
         pltpu.make_async_copy(win_ref, win.at[mine], load_sem.at[0]),
         pltpu.make_async_copy(wpo_ref, wpo.at[mine], load_sem.at[1]),
         pltpu.make_async_copy(wup_ref, sup, load_sem.at[2]),
-        pltpu.make_async_copy(wup_ref.at[:, part_cols], wup.at[mine], load_sem.at[3]),
+        pltpu.make_async_copy(wup_ref.at[:, part_cols], wup.at[mine, pl.ds(0, fh)], load_sem.at[3]),
         pltpu.make_async_copy(wdn_ref, sdn, load_sem.at[4]),
-        pltpu.make_async_copy(wdn_ref.at[:, part_cols], wdn.at[mine], load_sem.at[5]),
+        pltpu.make_async_copy(wdn_ref.at[:, part_cols], wdn.at[mine, pl.ds(0, fh)], load_sem.at[5]),
     ]
+    if spare:
+        for k, (src, dst) in enumerate(((wup_ref, wup), (wdn_ref, wdn))):
+            loads.append(pltpu.make_async_copy(
+                src.at[:, pl.ds(2 * fh, spare)], dst.at[mine, pl.ds(fh, spare)], load_sem.at[7 + k]))
     x_load = pltpu.make_async_copy(x_ref, xfull.at[t], load_sem.at[6])
     x_load.start()
     for copy in loads:
@@ -214,9 +260,9 @@
 
     x_load.wait()
     for q in range(lanes):
-        x_copy(q).start()
         for k in range(2):
             g_copy(q, k).start()
+            x_copy(q, k).start()
     loads[0].wait()
     own_start(WIN)
     spread_out(WIN)
@@ -227,8 +273,8 @@
     loads[3].wait()
     gfull[0, t] = ga_ref[...]
     gfull[1, t] = gb_ref[...]
-    loads[4].wait()
-    loads[5].wait()
+    for copy in loads[4:]:
+        copy.wait()
 
     rb = math.gcd(math.gcd(cut, rows - cut), 32)
 
@@ -258,7 +304,7 @@
 
             @pl.when(ahead if first else ~ahead)
             def _():
-                zsend(w, j).start()
+                zpush(w, j)
 
     edge = (z == 0) | (z == zn - 1)
     z_in(WIN, 1)
@@ -281,16 +327,19 @@
     y_in(WPO, 0)
     for j in near[:-1]:
         y_in(WIN, j)
-    with scope("xwait"):
-        for q in range(lanes):
-            x_copy(q).wait_recv()
-            for k in range(2):
-                g_copy(q, k).wait_recv()
-    with scope("norm1"):
-        blocks_of(first_norm)
-    wave(UP0, False)
-    zsends(UP0, [1])
-    own_start(UP0)
+    for k in range(2):
+        with scope("xwait"):
+            for q in range(lanes):
+                if k == 0:
+                    for v in range(2):
+                        g_copy(q, v).wait_recv()
+                x_copy(q, k).wait_recv()
+        with scope("norm1"):
+            blocks_of(first_norm, k * head, rows if k else head)
+        if k == 0:
+            wave(UP0, False)
+            zsends(UP0, [1])
+            own_start(UP0)
     y_in(WIN, near[-1])
     y_in(WPO, near[0])
     s_in(WIN)
@@ -384,16 +433,27 @@
     def _():
         zsends(DN, [1])
 
-    hb = math.gcd(fq, 512)
+    hb = min(fq, 512)
 
     def ff1(s, lo, hi):
-        def up(k, carry):
-            cs = pl.ds(pl.multiple_of(lo + k * hb, hb), hb)
+        def up(c0, cw):
+            cs = pl.ds(c0, cw)
             act = jnp.maximum(jnp.dot(middle[s], wup[:, cs], preferred_element_type=f32), 0.0)
             hidden[slot(s), cs] = (act * act).astype(bf16)
+
+        def step(k, carry):
+            up(pl.multiple_of(lo + k * hb, 128), hb)
             return carry
+
         with scope("ff1"):
-            lax.fori_loop(0, (hi - lo) // hb, up, 0)
+            whole = (hi - lo) // hb
+            lax.fori_loop(0, whole, step, 0)
+            if (hi - lo) % hb:
+                up(lo + whole * hb, (hi - lo) % hb)
+            if spare and hi == fh:
+                @pl.when(taker)
+                def _():
+                    up(fh, spare)
 
     def pass_on(h):
         a_back = middle.at[1 - role, half(h), slab]
@@ -416,22 +476,24 @@
 
     landed = []
 
-    def down(j, s, kept, start=True):
+    def down(j, s, kept):
         g = group(j, s)
         which = role if kept else 1 - role
         if (j, s) not in landed:
             landed.append((j, s))
             with scope(f"dshare{j}_{s}"):
-                share(DN, j, s).wait_recv()
+                s_wait(DN, j, s)
         with scope("ff2"):
-            w = wdn[pl.ds(pl.multiple_of(g * rc, rc), rc), :]
-            part[g, slot(which), :] = nt_dot(hidden[slot(which), :], w).astype(bf16)
-
-        if start:
-            hand(j, s, kept)
-
-    def hand(j, s, kept):
-        g = group(j, s)
+            rhs = pl.ds(pl.multiple_of(g * rc, rc), rc)
+
+            def product(depth):
+                part[g, slot(which), :] = nt_dot(hidden[slot(which), :depth], wdn[rhs, :depth]).astype(bf16)
+
+            if spare:
+                pl.when(taker)(lambda: product(fh + spare))
+                pl.when(~taker)(lambda: product(fh))
+            else:
+                product(fh)
 
         @pl.when(lax.div(g, per) != t)
         def _():
@@ -486,10 +548,10 @@
         zsends(DN, mids[1:])
 
     z_in(DN, far[0])
-    down(far[0], 0, True, False)
+    down(far[0], 0, True)
     blocks_of(residual)
     y_in(DN, 0)
-    down(0, 1, True, False)
+    down(0, 1, True)
 
     @pl.when(~edge)
     def _():
@@ -508,19 +570,17 @@
     ff1(1 - role, 0, fh)
     for ev in ((0, 0), (far[0], 0), (0, 1)):
         down(*ev, False)
-    for ev in ((far[0], 0), (0, 1)):
-        hand(*ev, True)
     pending = [(0, 0), (far[0], 0), (0, 1)]
     done = []
     for k in range(len(far)):
         if k and k + 1 < len(far):
             z_in(DN, far[k + 1])
         y_in(DN, far[k])
-        both(far[k], 1)
-        pending.append((far[k], 1))
-        if k + 1 < len(far):
-            both(far[k + 1], 0)
-            pending.append((far[k + 1], 0))
+        late = [(far[k + 1], 0)] if k + 1 < len(far) else []
+        for ev in late + [(far[k], 1)]:
+            both(*ev)
+            pending.append(ev)
+        if late:
             for ev in pending[:2 + k]:
                 fold(*ev)
             done += pending[:2 + k]
@@ -545,8 +605,8 @@
 
     def drain():
         for q in range(lanes):
-            x_copy(q).wait_send()
             for k in range(2):
+                x_copy(q, k).wait_send()
                 g_copy(q, k).wait_send()
             for h in range(2):
                 m_copy(q, h).wait_send()
@@ -568,10 +628,10 @@
             return carry
 
         lax.fori_loop(0, per, folded, 0)
-        for w in range(len(streams)):
+        for w in range(len(streams) if spare else len(streams) - 2):
             for j in order:
                 if j == 1 or (j and w not in (WIN, WPO)):
-                    zsend(w, j).wait_send()
+                    having(w, central(across(j)), lambda: zsend(w, j).wait_send())
                 elif j:
                     @pl.when(gate(across(j), z))
                     def _():
@@ -580,9 +640,12 @@
                     @pl.when(gate(z, across(j)))
                     def _():
                         relay(w, j).wait_send()
-                yfwd(w, j).wait_send()
-                share(w, j, 0).wait_send()
-                share(w, j, 1).wait_send()
+
+                def rest():
+                    yfwd(w, j).wait_send()
+                    share(w, j, 0).wait_send()
+                    share(w, j, 1).wait_send()
+                having(w, taker, rest)
 
     stat[...] = jnp.transpose(moments[0])[0:8, :]
     for q in range(lanes):
@@ -617,7 +680,7 @@
     rows, feat = tokens.shape
     own, cin = w_in.shape
     ffw = w_ff1.shape[1]
-    fh = ffw // 2
+    fh = (ffw + ffw // 16 // 256 * 256) // 2
     width = feat * tps
     n = zn * 2
     per = n // tps
@@ -654,9 +717,9 @@
             pltpu.VMEM((8, rows), f32),
             pltpu.VMEM((lanes, 8, rows), f32),
             pltpu.VMEM((rows, cin), f32),
-            dma((7,)),
-            dma((5, zn)), dma((2, zn)), dma((5, zn)), dma((5, zn)), dma((5, zn)), dma((5, zn, 2)), dma((5, zn, 2)),
-            dma((lanes,)), dma((lanes,)), dma((lanes, 2)), dma((lanes, 2)),
+            dma((9,)),
+            dma((8, zn)), dma((2, zn)), dma((8, zn)), dma((8, zn)), dma((8, zn)), dma((8, zn, 2)), dma((8, zn, 2)),
+            dma((lanes, 2)), dma((lanes, 2)), dma((lanes, 2)), dma((lanes, 2)),
             dma((lanes, 2)), dma((lanes, 2)), dma((2,)), dma((2,)), dma((lanes, 2)), dma((lanes, 2)),
             dma((n, 2)), dma((lanes, per, 2)), dma((per,)), dma((per,)), dma((lanes,)), dma((lanes,)),
         ],

time: 156 us -> 151 us (0.968)
  Pallas kernels: 154 us -> 149 us
    pallas_call x1, Pallas kernels: 154 us -> 149 us  [local(): pl.pallas_call(functools.partial(kernel, zn, tps), out_shape=jax.ShapeDty...]
where the time goes in v4:
time: 151 us
  Pallas kernels  149 us (99%)
  local copies, waits for them, and re-layouts  2.06 us (1%)
    pallas_call x1, Pallas kernels, local(): pl.pallas_call(functools.partial(kernel, zn, tps), out_shape=jax.ShapeDty...  149 us

profile of v4, /device:TPU:0, one launch (start us, length us, event | category | flops | bytes accessed | tf_op | source)
XLA Modules:
  0.0 151.1 jit_solution(16878895366123116983)
XLA Ops:
  0.0 149.1 %shard_map.91 = bf16[384,1024]{1,0:T(8,128)(2,1)} custom-call(bf16[384,1024]{1,0:T(8,128)(2,1)} %x_ref.1, f32[1,1024]{1,0:T(1,128)} %bitcast.4, f32[1,1024]{1,0:T(1,128)} %bitcast.5, f32[1,512]{1,0:T(1,128)} %bitcast.7, f32[1,1024]{1,0:T(1,128)} %bitcast.6, bf16[128,512]{1,0:T(8,128)(2,1)} %win_ref.1, bf16[128,512]{1,0:T(8,128)(2,1)} %wpo_ref.1, ...), custom_call_target="tpu_custom_call" | custom-call | tf_op jit(solution)/shard_map/pallas_call | solution.py:691
  149.1 2.1 %copy.11 = bf16[384,1024]{1,0:T(8,128)(2,1)} copy(bf16[384,1024]{1,0:T(8,128)(2,1)} %shard_map.91) | data formatting | bytes 1572864

commit v5 on v4

--- a/solution.py
+++ b/solution.py
@@ -24,7 +24,7 @@
     x_ref, ga_ref, gb_ref, scale_ref, gout_ref, win_ref, wpo_ref, wup_ref, wdn_ref, out_ref,
     win, wpo, wup, wdn, sup, sdn, xfull, gfull, mixed, mpart, mrecv, middle, hidden,
     part, precv, zpart, zrecv, total, moments, spread, stat, srecv, work,
-    load_sem, zs_sem, zq_sem, zr_sem, ys_sem, yr_sem, ss_sem, sr_sem, xs_sem, xr_sem, gs_sem, gr_sem,
+    load_sem, zs_sem, zq_sem, zr_sem, ys_sem, yr_sem, ss_sem, sr_sem, dr_sem, xs_sem, xr_sem, gs_sem, gr_sem,
     ms_sem, mr_sem, as_sem, ar_sem, fs_sem, fr_sem, rs_sem, rr_sem, ps_sem, pr_sem, ts_sem, tr_sem,
 ):
     i, t = lax.axis_index("fs"), lax.axis_index("tp")
@@ -105,15 +105,15 @@
             stage = sdn if ref is wdn else sup
             first = 2 * fh if w in extra else lax.rem(zd, 2) * fh + c0
             src = stage.at[:, pl.ds(pl.multiple_of(first, 128), cw)]
-        return remote(src, b, zs_sem.at[w, j], zr_sem.at[w, j], dev(zd, y, c), t)
+        return remote(src, b, zs_sem.at[w], zr_sem.at[w, j], dev(zd, y, c), t)
 
     def yfwd(w, j):
         b = block(w, across(j), y, c)
-        return remote(b, b, ys_sem.at[w, j], yr_sem.at[w, j], opp, t)
+        return remote(b, b, ys_sem.at[w], yr_sem.at[w, j], opp, t)
 
     def share(w, j, s):
         b = block(w, across(j), y if s == 0 else 1 - y, c)
-        return remote(b, b, ss_sem.at[w, j, s], sr_sem.at[w, j, s], sib, t)
+        return remote(b, b, ss_sem.at[w], dr_sem.at[j, s] if w in DN else sr_sem.at[w], sib, t)
 
     def parts(w):
         return w if isinstance(w, tuple) else (w,)
@@ -176,15 +176,26 @@
                 share(w, j, 1).start()
             having(w, taker, act)
 
-    def s_wait(ws, j, s):
-        for w in parts(ws):
-            having(w, taker, lambda: share(w, j, s).wait_recv())
+    def stretch(w, count):
+        ref, c0, cw = streams[w]
+        return ref.at[pl.ds(0, count * own), pl.ds(c0, cw)]
+
+    def d_wait(j, s):
+        def act(depth):
+            b = wdn.at[pl.ds(0, own), pl.ds(0, depth)]
+            remote(b, b, ss_sem.at[DN0], dr_sem.at[j, s], sib, t).wait_recv()
+
+        if spare:
+            pl.when(taker)(lambda: act(fh + spare))
+            pl.when(~taker)(lambda: act(fh))
+        else:
+            act(fh)
 
     def s_in(ws):
         with scope(f"s{parts(ws)[0]}"):
-            for j in order:
-                for s in range(2):
-                    s_wait(ws, j, s)
+            for w in parts(ws):
+                b = stretch(w, 2 * zn)
+                having(w, taker, lambda: remote(b, b, ss_sem.at[w], sr_sem.at[w], sib, t).wait_recv())
 
     head = rows * 3 // 4
 
@@ -435,11 +446,18 @@
 
     hb = min(fq, 512)
 
-    def ff1(s, lo, hi):
+    def ff1(s, lo, hi, h=None):
+        if h is None:
+            r0, count = 0, rows
+        else:
+            r0, count = ends[h], ends[h + 1] - ends[h]
+
         def up(c0, cw):
             cs = pl.ds(c0, cw)
-            act = jnp.maximum(jnp.dot(middle[s], wup[:, cs], preferred_element_type=f32), 0.0)
-            hidden[slot(s), cs] = (act * act).astype(bf16)
+            act = jnp.dot(middle[s, pl.ds(r0, count), :], wup[:, cs], preferred_element_type=f32)
+            act = jnp.maximum(act, 0.0)
+            to = pl.ds(pl.multiple_of(s * rows + r0, 16), count)
+            hidden[to, cs] = (act * act).astype(bf16)
 
         def step(k, carry):
             up(pl.multiple_of(lo + k * hb, 128), hb)
@@ -482,7 +500,7 @@
         if (j, s) not in landed:
             landed.append((j, s))
             with scope(f"dshare{j}_{s}"):
-                s_wait(DN, j, s)
+                d_wait(j, s)
         with scope("ff2"):
             rhs = pl.ds(pl.multiple_of(g * rc, rc), rc)
 
@@ -553,22 +571,27 @@
     y_in(DN, 0)
     down(0, 1, True)
 
+    def f_wait(h):
+        with scope("fwait"):
+            for q in range(lanes):
+                f_copy(q, h).wait_recv()
+
+    f_wait(0)
+    ff1(1 - role, 0, fh, 0)
+
     @pl.when(~edge)
     def _():
         z_in(DN, 1)
 
-    with scope("fwait"):
-        for h in range(2):
-            for q in range(lanes):
-                f_copy(q, h).wait_recv()
+    f_wait(1)
 
     @pl.when(edge)
     def _():
         zsends(DN, mids[1:])
         z_in(DN, 1)
 
-    ff1(1 - role, 0, fh)
-    for ev in ((0, 0), (far[0], 0), (0, 1)):
+    ff1(1 - role, 0, fh, 1)
+    for ev in ((far[0], 0), (0, 0), (0, 1)):
         down(*ev, False)
     pending = [(0, 0), (far[0], 0), (0, 1)]
     done = []
@@ -628,24 +651,27 @@
             return carry
 
         lax.fori_loop(0, per, folded, 0)
+        def gone(sem, w, count):
+            if count:
+                b = stretch(w, count)
+                remote(b, b, sem.at[w], zr_sem.at[w, 0], opp, t).wait_send()
+
         for w in range(len(streams) if spare else len(streams) - 2):
-            for j in order:
-                if j == 1 or (j and w not in (WIN, WPO)):
-                    having(w, central(across(j)), lambda: zsend(w, j).wait_send())
-                elif j:
-                    @pl.when(gate(across(j), z))
-                    def _():
-                        zsend(w, j).wait_send()
-
+            if w in extra:
+                pl.when(taker)(lambda: gone(zs_sem, w, zn // 2 - 1))
+                pl.when(~taker)(lambda: gone(zs_sem, w, zn // 2))
+            else:
+                gone(zs_sem, w, zn // 2 if w in (WIN, WPO) else zn - 1)
+
+            def rest():
+                gone(ys_sem, w, zn)
+                gone(ss_sem, w, 2 * zn)
+            having(w, taker, rest)
+            if w in (WIN, WPO):
+                for j in near[1:]:
                     @pl.when(gate(z, across(j)))
                     def _():
                         relay(w, j).wait_send()
-
-                def rest():
-                    yfwd(w, j).wait_send()
-                    share(w, j, 0).wait_send()
-                    share(w, j, 1).wait_send()
-                having(w, taker, rest)
 
     stat[...] = jnp.transpose(moments[0])[0:8, :]
     for q in range(lanes):
@@ -718,7 +744,7 @@
             pltpu.VMEM((lanes, 8, rows), f32),
             pltpu.VMEM((rows, cin), f32),
             dma((9,)),
-            dma((8, zn)), dma((2, zn)), dma((8, zn)), dma((8, zn)), dma((8, zn)), dma((8, zn, 2)), dma((8, zn, 2)),
+            dma((8,)), dma((2, zn)), dma((8, zn)), dma((8,)), dma((8, zn)), dma((8,)), dma((8,)), dma((zn, 2)),
             dma((lanes, 2)), dma((lanes, 2)), dma((lanes, 2)), dma((lanes, 2)),
             dma((lanes, 2)), dma((lanes, 2)), dma((2,)), dma((2,)), dma((lanes, 2)), dma((lanes, 2)),
             dma((n, 2)), dma((lanes, per, 2)), dma((per,)), dma((per,)), dma((lanes,)), dma((lanes,)),

time: 151 us -> 149 us (0.987)
  Pallas kernels: 149 us -> 146 us
    pallas_call x1, Pallas kernels: 149 us -> 146 us  [local(): pl.pallas_call(functools.partial(kernel, zn, tps), out_shape=jax.ShapeDty...]
where the time goes in v5:
time: 149 us
  Pallas kernels  146 us (98%)
  local copies, waits for them, and re-layouts  2.06 us (1%)
    pallas_call x1, Pallas kernels, local(): pl.pallas_call(functools.partial(kernel, zn, tps), out_shape=jax.ShapeDty...  146 us

profile of v5, /device:TPU:0, one launch (start us, length us, event | category | flops | bytes accessed | tf_op | source)
XLA Modules:
  0.0 148.5 jit_solution(4285251154373125442)
XLA Ops:
  0.0 146.5 %shard_map.91 = bf16[384,1024]{1,0:T(8,128)(2,1)} custom-call(bf16[384,1024]{1,0:T(8,128)(2,1)} %x_ref.1, f32[1,1024]{1,0:T(1,128)} %bitcast.4, f32[1,1024]{1,0:T(1,128)} %bitcast.5, f32[1,512]{1,0:T(1,128)} %bitcast.7, f32[1,1024]{1,0:T(1,128)} %bitcast.6, bf16[128,512]{1,0:T(8,128)(2,1)} %win_ref.1, bf16[128,512]{1,0:T(8,128)(2,1)} %wpo_ref.1, ...), custom_call_target="tpu_custom_call" | custom-call | tf_op jit(solution)/shard_map/pallas_call | solution.py:717
  146.5 2.1 %copy.11 = bf16[384,1024]{1,0:T(8,128)(2,1)} copy(bf16[384,1024]{1,0:T(8,128)(2,1)} %shard_map.91) | data formatting | bytes 1572864

commit v6 on v5

--- a/solution.py
+++ b/solution.py
@@ -558,6 +558,11 @@
                 total[gl] = total[gl] + (ff + zrecv[gl].astype(f32)).astype(bf16).astype(f32)
 
     down(0, 0, True)
+
+    @pl.when(edge)
+    def _():
+        z_in(DN, far[0])
+
     pass_on(1)
 
     @pl.when(~edge)
@@ -565,7 +570,11 @@
         zsends(DN, [1])
         zsends(DN, mids[1:])
 
-    z_in(DN, far[0])
+
+    @pl.when(~edge)
+    def _():
+        z_in(DN, far[0])
+
     down(far[0], 0, True)
     blocks_of(residual)
     y_in(DN, 0)

time: 149 us -> 149 us (level)
  no operation moved by 1% of the time
where the time goes in v6:
time: 149 us
  Pallas kernels  146 us (98%)
  local copies, waits for them, and re-layouts  2.06 us (1%)
    pallas_call x1, Pallas kernels, local(): pl.pallas_call(functools.partial(kernel, zn, tps), out_shape=jax.ShapeDty...  146 us

profile of v6, /device:TPU:0, one launch (start us, length us, event | category | flops | bytes accessed | tf_op | source)
XLA Modules:
  0.0 148.5 jit_solution(16713486088960692804)
XLA Ops:
  0.0 146.5 %shard_map.91 = bf16[384,1024]{1,0:T(8,128)(2,1)} custom-call(bf16[384,1024]{1,0:T(8,128)(2,1)} %x_ref.1, f32[1,1024]{1,0:T(1,128)} %bitcast.4, f32[1,1024]{1,0:T(1,128)} %bitcast.5, f32[1,512]{1,0:T(1,128)} %bitcast.7, f32[1,1024]{1,0:T(1,128)} %bitcast.6, bf16[128,512]{1,0:T(8,128)(2,1)} %win_ref.1, bf16[128,512]{1,0:T(8,128)(2,1)} %wpo_ref.1, ...), custom_call_target="tpu_custom_call" | custom-call | tf_op jit(solution)/shard_map/pallas_call | solution.py:726
  146.5 2.1 %copy.11 = bf16[384,1024]{1,0:T(8,128)(2,1)} copy(bf16[384,1024]{1,0:T(8,128)(2,1)} %shard_map.91) | data formatting | bytes 1572864
